TPU v7x, 32 devices: a whole 2x2x4 slice. The times are simulated.
32 devices in a mesh: grp: 2 (over y), sp: 4 (over z), tp: 4 (over x, core).
Axes of the slice: x: 2, y: 2, z: 4, core: 2. Of those that a mesh axis runs over, the one named last changes fastest.
Arguments:
- hidden_items: bfloat16 [1024, 4096], P(('grp', 'sp', 'tp')), parts along dimension 0, may hold values from -6 to 6
- sample_cond: bfloat16 [8192], P('grp'), parts along dimension 0, may hold values from -6 to 6
- prompt_items: bfloat16 [256, 4096], P(('grp', 'sp')), parts along dimension 0, may hold values from -6 to 6
- prompt_cond: bfloat16 [4096], replicated, may hold values from -6 to 6
- adjust_shifting: bfloat16 [4096, 4096], P('sp', 'tp'), may hold values from -0.125 to 0.125
- adjust_stretch: bfloat16 [4096, 4096], P('sp', 'tp'), may hold values from -0.125 to 0.125
- skip_valve: bfloat16 [4096, 4096], P('sp', 'tp'), may hold values from -0.125 to 0.125
- receiver_matrix: bfloat16 [4096, 2048], P(None, 'tp'), may hold values from -0.09375 to 0.09375
- address_matrix: bfloat16 [4096, 2048], P(None, 'tp'), may hold values from -0.09375 to 0.09375
- payload_matrix: bfloat16 [4096, 2048], P(None, 'tp'), may hold values from -0.09375 to 0.09375
- joint_lower_projector: bfloat16 [4096, 64], P('sp'), may hold values from -0.09375 to 0.09375
- fading_raise_matrix: bfloat16 [64, 2048], P(None, 'tp'), may hold values from -1.5 to 1.5
- step_raise_matrix: bfloat16 [64, 2048], P(None, 'tp'), may hold values from -1.5 to 1.5
- feature_fading: float32 [2048], P('tp'), may hold values from 0 to 0.1, as said below
- spike_logfade: float32 [1024, 32], P(('grp', 'sp'), 'tp'), parts along dimension 0, may hold values from 0 to 2
- group_standard_factor: float32 [2048], P('tp'), may hold values from 0.1 to 1.9
- emit_matrix: bfloat16 [2048, 4096], P('tp', 'sp'), may hold values from -0.125 to 0.125
Outputs:
- latent_out: bfloat16 [1024, 4096], P(('grp', 'sp', 'tp')), parts along dimension 0
There are 2 independent parts, one for each index of `grp`. A program takes and returns all parts, laid end to end along the dimension named above; an argument that names none is the same for every part. Nothing has to cross between parts.
Inputs may be any that keep to these rules, and one draw needn't show every extreme that they name: `feature_fading`: per-token decay rate of each channel.
All inputs are finite; a program needn't handle non-finite values.
Results may differ from a plain program's by a relative error of at most 0.015.
Values may be sent and summed in bfloat16 or wider, within the bound.
A program may use at most 128 MiB of HBM per device.

v0:
```python
import math

import jax
import jax.numpy as jnp
from jax import lax
from jax.sharding import PartitionSpec as P

ATTEND_WIDTH = 64


EXACT_MODE = lax.Precision.HIGHEST
EPS_ROW = 1e-05
EPS_HEAD = 0.00064
EPS_KEY = 1e-06
rate_shift = 5.0


def stored(value):
    return lax.optimization_barrier(value.astype(jnp.bfloat16))


def product(left, right):
    return jnp.dot(left, right, preferred_element_type=jnp.float32)


def batch_dot(left, right):
    return jnp.matmul(left, right, precision=EXACT_MODE)


def flipped(tensor):
    return jnp.swapaxes(tensor, -1, -2)


def modulate(rows, shifts, scales):
    values = rows.astype(jnp.float32)
    centre = jnp.mean(values, -1, keepdims=True)
    spread = jnp.mean(jnp.square(values - centre), -1, keepdims=True)
    normed = (values - centre) * lax.rsqrt(spread + EPS_ROW)
    return (normed * (1.0 + scales) + shifts).astype(jnp.bfloat16)


def both_ways(tensor):
    return jnp.stack([tensor, jnp.flip(tensor, axis=1)])


def chain_inputs(
    key_rows,
    value_rows,
    low_rows,
    query_rows,
    fading_raise_matrix,
    step_raise_matrix,
    feature_fading,
    surplus_entries,
):
    row_count = key_rows.shape[0]
    head_count = key_rows.shape[1] // ATTEND_WIDTH
    squashed = jnp.tanh(low_rows.astype(jnp.float32)).astype(jnp.bfloat16)
    logdecay = (
        -feature_fading * jax.nn.sigmoid(product(squashed, fading_raise_matrix)) - surplus_entries
    )
    learned = jax.nn.sigmoid(product(squashed, step_raise_matrix) - rate_shift)

    def by_head(tensor):
        return jnp.transpose(
            tensor.astype(jnp.float32).reshape(row_count, head_count, ATTEND_WIDTH), (1, 0, 2)
        )

    key_heads = by_head(key_rows)
    unit_keys = key_heads * lax.rsqrt(jnp.sum(key_heads * key_heads, -1, keepdims=True) + EPS_KEY)
    removal = unit_keys * by_head(learned)
    return tuple(
        (
            both_ways(tensor)
            for tensor in (
                by_head(logdecay),
                key_heads,
                by_head(value_rows),
                unit_keys,
                removal,
                by_head(query_rows),
            )
        )
    )


def sub_block(carried, inputs, reading):
    logdecay, key_heads, value_heads, unit_keys, removal, query_heads = inputs
    sub_len = logdecay.shape[-2]
    totals = jnp.cumsum(logdecay, axis=-2)
    inclusive = jnp.exp(totals)
    exclusive = jnp.exp(totals - logdecay)
    inverse = jnp.exp(-totals)
    probed = exclusive * unit_keys
    key_in = key_heads * inverse
    removal_in = removal * inverse
    places = lax.iota(jnp.int32, sub_len)
    strict = (places[:, None] > places[None, :]).astype(jnp.float32)
    system = batch_dot(probed, flipped(removal_in)) * strict + jnp.eye(sub_len, dtype=jnp.float32)
    right_side = batch_dot(probed, flipped(carried)) + batch_dot(
        batch_dot(probed, flipped(key_in)) * strict, value_heads
    )
    solved = jax.scipy.linalg.solve_triangular(system, right_side, lower=True, unit_diagonal=True)
    final_row = inclusive[..., -1:, :]
    ending = (
        carried * final_row
        + batch_dot(flipped(value_heads), key_in * final_row)
        - batch_dot(flipped(solved), removal_in * final_row)
    )
    if not reading:
        return (ending, jnp.zeros((), jnp.float32))
    weighted = inclusive * query_heads
    upto_mask = (places[:, None] >= places[None, :]).astype(jnp.float32)
    outputs = (
        batch_dot(weighted, flipped(carried))
        + batch_dot(batch_dot(weighted, flipped(key_in)) * upto_mask, value_heads)
        - batch_dot(batch_dot(weighted, flipped(removal_in)) * upto_mask, solved)
    )
    return (ending, outputs)


def run_chain(carried, inputs, reading):
    length = inputs[0].shape[-2]
    sub_len = math.gcd(64, length)

    def to_blocks(tensor):
        leading = tensor.shape[:-2]
        shaped = tensor.reshape(leading + (length // sub_len, sub_len, tensor.shape[-1]))
        return jnp.moveaxis(shaped, -3, 0)

    def advance(state_now, pieces):
        return sub_block(state_now, pieces, reading)

    ending, outputs = lax.scan(advance, carried, tuple((to_blocks(tensor) for tensor in inputs)))
    if reading:
        outputs = jnp.moveaxis(outputs, 0, -3)
        outputs = outputs.reshape(outputs.shape[:-3] + (length, outputs.shape[-1]))
    return (ending, outputs)


def body(
    hidden_items,
    sample_cond,
    prompt_items,
    prompt_cond,
    adjust_shifting,
    adjust_stretch,
    skip_valve,
    receiver_matrix,
    address_matrix,
    payload_matrix,
    joint_lower_projector,
    fading_raise_matrix,
    step_raise_matrix,
    feature_fading,
    spike_logfade,
    group_standard_factor,
    emit_matrix,
):
    width = hidden_items.shape[1]
    span_rows = adjust_shifting.shape[0]
    conditions = jnp.stack([sample_cond, prompt_cond])
    activated = jax.nn.silu(conditions.astype(jnp.float32)).astype(jnp.bfloat16)
    own_cols = lax.dynamic_slice_in_dim(activated, lax.axis_index("sp") * span_rows, span_rows, 1)
    part_shift = product(own_cols, adjust_shifting)
    part_scale = product(own_cols, adjust_stretch)
    part_gate = product(own_cols[:1], skip_valve)
    summed = lax.psum((part_shift, part_scale, part_gate), "sp")
    shifts, scales, gates = (
        lax.all_gather(summed[0], "tp", axis=1, tiled=True),
        lax.all_gather(summed[1], "tp", axis=1, tiled=True),
        lax.all_gather(summed[2], "tp", axis=1, tiled=True),
    )
    out_weight, down_weight = (
        lax.all_gather(emit_matrix, "sp", axis=1, tiled=True),
        lax.all_gather(joint_lower_projector, "sp", axis=0, tiled=True),
    )
    u_rows = modulate(hidden_items, shifts[0], scales[0])
    low_own = stored(product(u_rows, down_weight))
    joined = jnp.concatenate([u_rows, low_own], axis=1)
    portion = lax.all_gather(joined, "tp", axis=0, tiled=True)
    features = portion[:, :width]
    gathered = jnp.concatenate(
        [
            stored(product(features, receiver_matrix)),
            stored(product(features, address_matrix)),
            stored(product(features, payload_matrix)),
            portion[:, width:],
        ],
        axis=1,
    )
    head_cols = receiver_matrix.shape[1]
    head_count = head_cols // ATTEND_WIDTH
    ctx_mod = modulate(prompt_items, shifts[1], scales[1])
    ctx_keys, ctx_values, ctx_low = (
        lax.all_gather(stored(product(ctx_mod, address_matrix)), "sp", axis=0, tiled=True),
        lax.all_gather(stored(product(ctx_mod, payload_matrix)), "sp", axis=0, tiled=True),
        lax.all_gather(stored(product(ctx_mod, down_weight)), "sp", axis=0, tiled=True),
    )
    ctx_inputs = chain_inputs(
        ctx_keys,
        ctx_values,
        ctx_low,
        ctx_keys,
        fading_raise_matrix,
        step_raise_matrix,
        feature_fading,
        0.0,
    )
    zeroed = jnp.zeros((2, head_count, ATTEND_WIDTH, ATTEND_WIDTH), jnp.float32)
    ctx_state, _ = run_chain(zeroed, ctx_inputs, False)
    surplus_entries = jnp.repeat(spike_logfade, ATTEND_WIDTH, axis=1)
    lat_inputs = chain_inputs(
        gathered[:, head_cols : 2 * head_cols],
        gathered[:, 2 * head_cols : 3 * head_cols],
        gathered[:, 3 * head_cols :],
        gathered[:, :head_cols],
        fading_raise_matrix,
        step_raise_matrix,
        feature_fading,
        surplus_entries,
    )
    identity_maps = jnp.broadcast_to(
        jnp.eye(ATTEND_WIDTH, dtype=jnp.float32), (2, head_count, ATTEND_WIDTH, ATTEND_WIDTH)
    )
    augmented = jnp.concatenate([jnp.zeros_like(identity_maps), identity_maps], axis=2)
    padded_values = jnp.concatenate([lat_inputs[2], jnp.zeros_like(lat_inputs[2])], axis=3)
    ending, _ = run_chain(augmented, lat_inputs[:2] + (padded_values,) + lat_inputs[3:], False)
    offsets = ending[:, :, :ATTEND_WIDTH]
    factors = ending[:, :, ATTEND_WIDTH:]
    every = lax.all_gather(
        jnp.stack([factors, offsets])[None].astype(jnp.bfloat16), "sp", axis=0, tiled=True
    ).astype(jnp.float32)
    own_index = lax.axis_index("sp")
    shards = every.shape[0]

    def walk_state(carried, item):
        number, forward_map, backward_map = item
        moved_ahead = batch_dot(carried[0], forward_map[0]) + forward_map[1]
        moved_behind = batch_dot(carried[1], backward_map[0]) + backward_map[1]
        ahead_now = jnp.where(number < own_index, moved_ahead, carried[0])
        behind_now = jnp.where(shards - 1 - number > own_index, moved_behind, carried[1])
        return ((ahead_now, behind_now), jnp.zeros((), jnp.float32))

    numbers = lax.iota(jnp.int32, shards)
    walked, _ = lax.scan(
        walk_state,
        (ctx_state[0], ctx_state[1]),
        (numbers, every[:, :, 0], jnp.flip(every[:, :, 1], axis=0)),
    )
    starting = jnp.stack([walked[0], walked[1]])
    _, outputs = run_chain(starting, lat_inputs, True)
    combined = outputs[0] + jnp.flip(outputs[1], axis=1)
    centre = jnp.mean(combined, -1, keepdims=True)
    spread = jnp.mean(jnp.square(combined - centre), -1, keepdims=True)
    gains = group_standard_factor.reshape(head_count, 1, ATTEND_WIDTH)
    normed = (combined - centre) * lax.rsqrt(spread + EPS_HEAD) * gains
    row_total = combined.shape[1]
    normed = jnp.transpose(normed, (1, 0, 2)).reshape(row_total, head_cols).astype(jnp.bfloat16)
    mixed_sum = lax.psum_scatter(
        product(normed, out_weight).astype(jnp.bfloat16), "tp", scatter_dimension=0, tiled=True
    ).astype(jnp.float32)
    return (hidden_items.astype(jnp.float32) + gates[0] * mixed_sum).astype(jnp.bfloat16)


def solution(mesh):
    placed = (
        P(("grp", "sp", "tp"), None),
        P("grp"),
        P(("grp", "sp"), None),
        P(),
        P("sp", "tp"),
        P("sp", "tp"),
        P("sp", "tp"),
        P(None, "tp"),
        P(None, "tp"),
        P(None, "tp"),
        P("sp", None),
        P(None, "tp"),
        P(None, "tp"),
        P("tp"),
        P(("grp", "sp"), "tp"),
        P("tp"),
        P("tp", "sp"),
    )
    return jax.shard_map(
        body, mesh=mesh, in_specs=placed, out_specs=P(("grp", "sp", "tp"), None), check_vma=False
    )
```

profile of v0, /device:TPU:0, one launch (start us, length us, event | category | flops | bytes accessed | tf_op | source)
XLA Modules:
  0.0 872.7 jit_solution(15902612985290796414)
XLA Ops:
  6.5 17.7 %all_gather.33 = bf16[4096,64]{0,1:T(8,128)(2,1)S(1)} all-gather(bf16[1024,64]{0,1:T(8,128)(2,1)} %param.37), channel_id=1, replica_groups=mesh['grp'=2,'sp'=4,'tp'=4] {'sp'}, dimensions={0}, use_global_device_ids=true | all-gather | bytes 655360 | tf_op jit(solution)/shard_map/all_gather | solution.py:176
  28.4 20.3 %all-reduce.2 = (f32[2,1024]{1,0:T(2,128)S(1)}, f32[2,1024]{1,0:T(2,128)S(1)}, f32[1,1024]{1,0:T(1,128)}) all-reduce(f32[2,1024]{1,0:T(2,128)S(1)} %fusion.138, f32[2,1024]{1,0:T(2,128)S(1)} %fusion.137, f32[1,1024]{1,0:T(1,128)S(1)} %fusion.128), channel_id=1, replica_groups=mesh['grp'=2,'sp'=4,'tp'=4] {'sp'}, use_global_device_ids=true, to_apply=%region_4.5 | all-reduce | flops 5120 | bytes 40960 | tf_op jit(solution)/shard_map/psum | solution.py:168
  48.6 5.2 all_gather.32
  53.8 5.2 all_gather.31
  61.3 14.7 %all-gather.4.cloned.1.call-done = bf16[128,4160]{1,0:T(8,128)(2,1)} async-done(((bf16[32,4160]{1,0:T(8,128)(2,1)}), bf16[128,4160]{1,0:T(8,128)(2,1)}) %all-gather.4.cloned.1.call-update) | async-done | bytes 1064976 | tf_op jit(solution)/shard_map/all_gather | solution.py:181
  78.7 2.9 convolution_convert_fusion.2
  89.0 2.9 convolution_convert_fusion.3
  94.7 2.1 stack.163
  96.8 2.5 maximum_bitcast_fusion.5
  99.4 2.4 maximum_bitcast_fusion.6
  101.8 190.7 %while.45 = (s32[]{:T(128)}, f32[2,8,128,64]{2,3,1,0:T(8,128)S(1)}, f32[2,2,8,64,64]{4,2,3,1,0:T(8,128)S(1)}, f32[2,2,8,64,128]{4,3,0,2,1:T(8,128)}, f32[2,2,8,6...) while((s32[]{:T(128)}, f32[2,8,128,64]{2,3,1,0:T(8,128)S(1)}, ...), condition=%wide.region_14.16_spmd, body=%wide.region_12.15_spmd.sunk | while | flops 609448000 | bytes 21115560 | solution.py:134
  102.2 2.6 constant_dynamic-slice_fusion.13
  106.3 2.3 broadcast_multiply_fusion.10
  114.1 80.0 %custom-call.15 = f32[2,8,1,64,64]{3,4,2,1,0:T(8,128)} custom-call(f32[2,8,1,64,64]{4,3,2,1,0:T(8,128)} %fusion.268), custom_call_target="InvertDiagBlocksLowerTriangular" | custom-call | tf_op jit(solution)/shard_map/while/body/eval_jaxpr/jit(_solve_triangular)/vmap(vmap())/triangular_solve | solution.py:103
  197.4 2.6 constant_dynamic-slice_fusion.13
  201.5 2.3 broadcast_multiply_fusion.10
  209.4 80.0 %custom-call.15 = f32[2,8,1,64,64]{3,4,2,1,0:T(8,128)} custom-call(f32[2,8,1,64,64]{4,3,2,1,0:T(8,128)} %fusion.268), custom_call_target="InvertDiagBlocksLowerTriangular" | custom-call | tf_op jit(solution)/shard_map/while/body/eval_jaxpr/jit(_solve_triangular)/vmap(vmap())/triangular_solve | solution.py:103
  295.2 13.4 %all_gather.34 = bf16[128,64]{1,0:T(8,128)(2,1)S(1)} all-gather(bf16[32,64]{1,0:T(8,128)(2,1)S(1)} %convolution_convert_fusion.7), channel_id=1, replica_groups=mesh['grp'=2,'sp'=4,'tp'=4] {'sp'}, dimensions={0}, use_global_device_ids=true | all-gather | bytes 20480 | tf_op jit(solution)/shard_map/all_gather | solution.py:198
  310.3 3.1 convolution_convert_fusion.4
  313.5 28.0 %all_gather.36 = bf16[128,512]{1,0:T(8,128)(2,1)S(1)} all-gather(bf16[32,512]{1,0:T(8,128)(2,1)S(1)} %convolution_convert_fusion.4), channel_id=1, replica_groups=mesh['grp'=2,'sp'=4,'tp'=4] {'sp'}, dimensions={0}, use_global_device_ids=true | all-gather | bytes 163840 | tf_op jit(solution)/shard_map/all_gather | solution.py:196
  342.8 3.1 convolution_convert_fusion.5
  345.9 15.7 %all_gather.35 = bf16[128,512]{1,0:T(8,128)(2,1)} all-gather(bf16[32,512]{1,0:T(8,128)(2,1)S(1)} %convolution_convert_fusion.5), channel_id=1, replica_groups=mesh['grp'=2,'sp'=4,'tp'=4] {'sp'}, dimensions={0}, use_global_device_ids=true | all-gather | bytes 163840 | tf_op jit(solution)/shard_map/all_gather | solution.py:197
  370.6 2.1 stack.139
  379.0 2.7 maximum_bitcast_fusion.1
  381.7 200.8 %while.48 = (s32[]{:T(128)}, f32[2,8,64,64]{3,2,1,0:T(8,128)}, f32[2,2,8,64,64]{4,2,3,1,0:T(8,128)}, f32[2,2,8,64,64]{3,0,4,2,1:T(2,128)}, f32[2,2,8,64,64]{3,0,...) while((s32[]{:T(128)}, f32[2,8,64,64]{3,2,1,0:T(8,128)}, ...), condition=%wide.region_8.10_spmd.clone, body=%wide.region_6.9_spmd.clone.sunk | while | flops 357986368 | bytes 14558924 | solution.py:134
  385.0 3.7 constant_dynamic-slice_fusion.17
  397.8 80.0 %custom-call.17 = f32[2,8,1,64,64]{3,4,2,1,0:T(8,128)} custom-call(f32[2,8,1,64,64]{4,3,2,1,0:T(8,128)} %fusion.316), custom_call_target="InvertDiagBlocksLowerTriangular" | custom-call | tf_op jit(solution)/shard_map/while/body/eval_jaxpr/jit(_solve_triangular)/vmap(vmap())/triangular_solve | solution.py:103
  477.8 2.2 fusion.317
  484.8 3.6 constant_dynamic-slice_fusion.17
  489.7 2.7 convolution_add_fusion.21
  498.7 80.0 %custom-call.17 = f32[2,8,1,64,64]{3,4,2,1,0:T(8,128)} custom-call(f32[2,8,1,64,64]{4,3,2,1,0:T(8,128)} %fusion.316), custom_call_target="InvertDiagBlocksLowerTriangular" | custom-call | tf_op jit(solution)/shard_map/while/body/eval_jaxpr/jit(_solve_triangular)/vmap(vmap())/triangular_solve | solution.py:103
  578.7 2.2 fusion.317
  586.3 2.9 convolution_convert_fusion.1
  594.0 2.0 convert_element_type.164
  596.1 2.3 slice_bitcast_fusion.1
  598.4 3.2 rev.51
  601.6 19.2 %while.46 = (s32[]{:T(128)}, f32[8,64,64]{1,2,0:T(8,128)S(1)}, f32[8,64,64]{1,2,0:T(8,128)S(1)}, s32[4]{0:T(128)S(1)}, s32[]{:T(128)}, /*index=5*/f32[4,2,8,64,6...) while((s32[]{:T(128)}, f32[8,64,64]{1,2,0:T(8,128)S(1)}, ...), condition=%wide.region_16.18_spmd, body=%wide.region_15.17_spmd.sunk | while | flops 50462724 | bytes 2887851 | solution.py:246
  621.2 211.6 %while.47 = (s32[]{:T(128)}, f32[2,8,64,64]{3,2,1,0:T(8,128)S(1)}, f32[2,2,8,64,64]{4,3,2,1,0:T(8,128)}, f32[2,2,8,64,64]{4,2,3,1,0:T(8,128)S(1)}, f32[2,2,8,64,...) while((s32[]{:T(128)}, f32[2,8,64,64]{3,2,1,0:T(8,128)S(1)}, ...), condition=%wide.region_19.21_spmd, body=%wide.region_17.20_spmd.sunk | while | flops 610111552 | bytes 35055476 | solution.py:134
  625.6 2.1 constant_dynamic-slice_fusion.15
  637.7 79.4 %custom-call.16 = f32[2,8,1,64,64]{3,4,2,1,0:T(8,128)S(1)} custom-call(f32[2,8,1,64,64]{4,3,2,1,0:T(8,128)} %fusion.296), custom_call_target="InvertDiagBlocksLowerTriangular" | custom-call | tf_op jit(solution)/shard_map/while/body/eval_jaxpr/jit(_solve_triangular)/vmap(vmap())/triangular_solve | solution.py:103
  717.0 2.0 fusion.297
  719.1 3.0 convolution_subtract_fusion.8
  731.2 2.1 constant_dynamic-slice_fusion.15
  743.2 79.4 %custom-call.16 = f32[2,8,1,64,64]{3,4,2,1,0:T(8,128)S(1)} custom-call(f32[2,8,1,64,64]{4,3,2,1,0:T(8,128)} %fusion.296), custom_call_target="InvertDiagBlocksLowerTriangular" | custom-call | tf_op jit(solution)/shard_map/while/body/eval_jaxpr/jit(_solve_triangular)/vmap(vmap())/triangular_solve | solution.py:103
  824.7 3.0 convolution_subtract_fusion.8
  835.7 4.1 convolution_convert_fusion
  839.9 5.2 all_gather.30
  845.1 18.9 %reduce-scatter.2.cloned.1.call-done = bf16[32,4096]{1,0:T(8,128)(2,1)} async-done(((bf16[128,4096]{1,0:T(8,128)(2,1)}), bf16[32,4096]{1,0:T(8,128)(2,1)}) %reduce-scatter.2.cloned.1.call-update) | async-done | bytes 262160 | tf_op jit(solution)/shard_map/reduce_scatter | solution.py:260
  (367 shorter events, 153.7 us)
Async XLA Ops:
  6.5 19.2 %copy-start = (bf16[1024,1024]{1,0:T(8,128)(2,1)S(1)}, bf16[1024,1024]{1,0:T(8,128)(2,1)}, u32[]{:S(2)}) copy-start(bf16[1024,1024]{1,0:T(8,128)(2,1)} %param.31) | copy-start | bytes 6291460
  6.5 69.5 %all-gather.4.cloned.1.call-start = ((), (), s32[]{:S(2)}) async-start(), calls=%async_computation.1 | async-start | bytes 1351680 | tf_op jit(solution)/shard_map/all_gather | solution.py:181
  24.2 35.4 %copy-start.21 = (bf16[4096,64]{0,1:T(8,128)(2,1)}, bf16[4096,64]{0,1:T(8,128)(2,1)S(1)}, u32[]{:S(2)}) copy-start(bf16[4096,64]{0,1:T(8,128)(2,1)S(1)} %all_gather.33) | copy-start | bytes 1572868
  25.8 2.2 copy-start.24
  27.3 31.7 %copy-start.17 = (bf16[32,4096]{1,0:T(8,128)(2,1)S(1)}, bf16[32,4096]{1,0:T(8,128)(2,1)}, u32[]{:S(2)}) copy-start(bf16[32,4096]{1,0:T(8,128)(2,1)} %param.27) | copy-start | bytes 786436
  28.0 32.8 %copy-start.49 = (f32[512]{0:T(512)S(1)}, f32[512]{0:T(512)}, u32[]{:S(2)}) copy-start(f32[512]{0:T(512)} %param.40) | copy-start | bytes 6148
  28.0 32.9 %copy-start.46 = (f32[128,8]{0,1:T(8,128)S(1)}, f32[128,8]{0,1:T(8,128)}, u32[]{:S(2)}) copy-start(f32[128,8]{0,1:T(8,128)} %param.41) | copy-start | bytes 12292
  59.7 16.3 %copy-start.50 = (bf16[64,512]{1,0:T(8,128)(2,1)S(1)}, bf16[64,512]{1,0:T(8,128)(2,1)}, u32[]{:S(2)}) copy-start(bf16[64,512]{1,0:T(8,128)(2,1)} %param.38) | copy-start | bytes 196612
  60.8 533.3 %all-gather.6.cloned.1.call-start = ((), (), s32[]{:S(2)}) async-start(), calls=%async_computation.2 | async-start | bytes 2621440 | tf_op jit(solution)/shard_map/all_gather | solution.py:231
  61.1 17.3 %copy-start.51 = (bf16[64,512]{1,0:T(8,128)(2,1)S(1)}, bf16[64,512]{1,0:T(8,128)(2,1)}, u32[]{:S(2)}) copy-start(bf16[64,512]{1,0:T(8,128)(2,1)} %param.39) | copy-start | bytes 196612
  76.0 2.4 copy-start.14
  92.5 4.3 copy-start.29
  92.5 4.3 copy-start.32
  96.8 2.5 copy-start.30
  96.8 2.5 copy-start.33
  96.8 2.5 copy-start.39
  96.8 2.5 copy-start.40
  106.3 2.3 copy-start.10
  112.2 84.0 %copy-start.9 = (f32[2,8,64,64]{3,1,2,0:T(8,128)S(1)}, f32[2,8,64,64]{3,1,2,0:T(8,128)}, u32[]{:S(2)}) copy-start(f32[2,8,64,64]{3,1,2,0:T(8,128)} %get-tuple-element.558) | copy-start | bytes 786436 | tf_op jit(solution)/shard_map/while
  201.5 2.3 copy-start.10
  207.4 84.0 %copy-start.9 = (f32[2,8,64,64]{3,1,2,0:T(8,128)S(1)}, f32[2,8,64,64]{3,1,2,0:T(8,128)}, u32[]{:S(2)}) copy-start(f32[2,8,64,64]{3,1,2,0:T(8,128)} %get-tuple-element.558) | copy-start | bytes 786436 | tf_op jit(solution)/shard_map/while
  292.5 2.3 copy-start.22
  293.6 542.0 %all-gather.8.cloned.1.call-start = ((), (), s32[]{:S(2)}) async-start(), calls=%async_computation.3 | async-start | bytes 5242880 | tf_op jit(solution)/shard_map/all_gather | solution.py:175
  294.4 569.6 %reduce-scatter.2.cloned.1.call-start = ((), (), s32[]{:S(2)}) async-start(), calls=%async_computation.4 | async-start | bytes 1310720 | tf_op jit(solution)/shard_map/reduce_scatter | solution.py:260
  294.9 15.2 %copy-start.52 = (bf16[64,512]{1,0:T(8,128)(2,1)S(1)}, bf16[64,512]{1,0:T(8,128)(2,1)}, u32[]{:S(2)}) copy-start(bf16[64,512]{1,0:T(8,128)(2,1)} %param.39) | copy-start | bytes 196612
  361.5 6.2 copy-start.41
  367.6 5.1 copy-start.43
  376.8 2.3 copy-start.36
  395.8 84.1 %copy-start.8 = (f32[2,8,64,64]{3,2,1,0:T(8,128)S(1)}, f32[2,8,64,64]{3,2,1,0:T(8,128)}, u32[]{:S(2)}) copy-start(f32[2,8,64,64]{3,2,1,0:T(8,128)} %convolution_add_fusion.21) | copy-start | bytes 786436 | tf_op jit(solution)/shard_map/while
  489.7 2.7 copy-start.5
  496.8 84.1 %copy-start.8 = (f32[2,8,64,64]{3,2,1,0:T(8,128)S(1)}, f32[2,8,64,64]{3,2,1,0:T(8,128)}, u32[]{:S(2)}) copy-start(f32[2,8,64,64]{3,2,1,0:T(8,128)} %convolution_add_fusion.21) | copy-start | bytes 786436 | tf_op jit(solution)/shard_map/while
  582.5 3.8 copy-start.15
  589.2 2.3 copy-start.25
  589.2 2.3 copy-start.26
  621.4 3.6 copy-start.13
  623.2 2.4 copy-start.11
  623.2 2.4 copy-start.12
  719.1 4.1 copy-start.7
  723.2 2.1 copy-start.44
  724.1 2.8 copy-start.4
  727.0 3.6 copy-start.13
  728.8 2.4 copy-start.11
  728.8 2.4 copy-start.12
  824.7 4.1 copy-start.7
  829.7 2.8 copy-start.4
  835.7 4.2 copy-start.47
  835.7 28.3 %copy-start.18 = (bf16[32,4096]{1,0:T(8,128)(2,1)S(1)}, bf16[32,4096]{1,0:T(8,128)(2,1)}, u32[]{:S(2)}) copy-start(bf16[32,4096]{1,0:T(8,128)(2,1)} %param.27) | copy-start | bytes 786436
  835.7 30.0 %copy-start.1 = (bf16[1024,1024]{1,0:T(8,128)(2,1)S(1)}, bf16[1024,1024]{1,0:T(8,128)(2,1)}, u32[]{:S(2)}) copy-start(bf16[1024,1024]{1,0:T(8,128)(2,1)} %param.31) | copy-start | bytes 6291460
  (23 other events, 37.2 us)
Sparse Core Ops, SparseCore 0:
  60.9 15.0 all-gather.3
  293.8 47.8 all-gather.5
  343.3 80.1 all-gather.7
  840.0 23.9 reduce-scatter.1
where the time goes:
time: 881 us; the launch traced here: 873 us
  other arithmetic  511 us (58%)
  blocking collectives  111 us (13%)
  matrix products  110 us (12%)
  local copies, waits for them, and re-layouts  85.3 us (10%)
  waiting for transfers between devices  34.4 us (4%)
  between operations  14.4 us (2%)
    another operation x18, other arithmetic, sub_block(): jax.scipy.linalg.solve_triangular(system, right_side, lower=True, unit_di...  479 us
    dot_general x54, matrix products, batch_dot(): return jnp.matmul(left, right, precision=EXACT_MODE)  74.9 us
    dynamic_slice x22, local copies, waits for them, and re-layouts, run_chain(): lax.scan(advance, carried, tuple((to_blocks(tensor) for tensor in inputs)))  32.4 us
    all_gather x1, blocking collectives, body(): lax.all_gather(stored(product(ctx_mod, address_matrix)), 'sp', axis=0, ti...  28 us
    another operation x22, local copies, waits for them, and re-layouts, both_ways(): return jnp.stack([tensor, jnp.flip(tensor, axis=1)])  24.3 us
    dot_general x15, matrix products, product(): return jnp.dot(left, right, preferred_element_type=jnp.float32)  22.3 us
    psum x1, blocking collectives, body(): summed = lax.psum((part_shift, part_scale, part_gate), 'sp')  20.3 us
    reduce_scatter x1, waiting for transfers between devices, body(): lax.psum_scatter(product(normed, out_weight).astype(jnp.bfloat16), 'tp',...  18.9 us
  transfers between devices with their start and end apart: 4, of which 2 were waited for; matrix products, arithmetic and copies ran while one was open for 54% of the time, Pallas kernels for 0%

commit v1 on v0

v1 whole, which is shorter than its diff:
```python
import functools
import math

import jax
import jax.numpy as jnp
from jax import lax
from jax.experimental import pallas as pl
from jax.experimental.pallas import tpu as pltpu
from jax.sharding import PartitionSpec as P

ATTEND_WIDTH = 64
PAIR = 2 * ATTEND_WIDTH

EXACT_MODE = lax.Precision.HIGHEST
EPS_ROW = 1e-05
EPS_HEAD = 0.00064
EPS_KEY = 1e-06
rate_shift = 5.0


def stored(value):
    return lax.optimization_barrier(value.astype(jnp.bfloat16))


def product(left, right):
    return jnp.dot(left, right, preferred_element_type=jnp.float32)


def modulate(rows, shifts, scales):
    values = rows.astype(jnp.float32)
    centre = jnp.mean(values, -1, keepdims=True)
    spread = jnp.mean(jnp.square(values - centre), -1, keepdims=True)
    normed = (values - centre) * lax.rsqrt(spread + EPS_ROW)
    return (normed * (1.0 + scales) + shifts).astype(jnp.bfloat16)


def low_dot(left, right):
    return jnp.dot(
        left.astype(jnp.bfloat16), right.astype(jnp.bfloat16), preferred_element_type=jnp.float32
    )


def low_dot_nt(left, right):
    return lax.dot_general(
        left.astype(jnp.bfloat16),
        right.astype(jnp.bfloat16),
        (((1,), (1,)), ((), ())),
        preferred_element_type=jnp.float32,
    )


def low_dot_tn(left, right):
    return lax.dot_general(
        left.astype(jnp.bfloat16),
        right.astype(jnp.bfloat16),
        (((0,), (0,)), ((), ())),
        preferred_element_type=jnp.float32,
    )


def exact_dot(left, right):
    return jnp.dot(left, right, precision=EXACT_MODE, preferred_element_type=jnp.float32)


def head_mask(size):
    row = lax.broadcasted_iota(jnp.int32, (size, size), 0)
    col = lax.broadcasted_iota(jnp.int32, (size, size), 1)
    return (row // ATTEND_WIDTH) == (col // ATTEND_WIDTH)


def token_features(keys, lows, raise_fading, raise_step, fading):
    squashed = jnp.tanh(lows.astype(jnp.float32)).astype(jnp.bfloat16)
    logdecay = -fading * jax.nn.sigmoid(product(squashed, raise_fading))
    learned = jax.nn.sigmoid(product(squashed, raise_step) - rate_shift)
    same_head = head_mask(PAIR).astype(jnp.float32)
    unit = keys * lax.rsqrt(exact_dot(keys * keys, same_head) + EPS_KEY)
    return unit, unit * learned, logdecay


def block_inverses(systems, uppers):
    size = systems[0].shape[0]
    row = lax.broadcasted_iota(jnp.int32, (size, size), 0)
    col = lax.broadcasted_iota(jnp.int32, (size, size), 1)
    eye = (row == col).astype(jnp.float32)
    inverses = None
    width = 1
    while width < size:
        merged = (row // (2 * width) == col // (2 * width)) & (row // width != col // width)
        pieces = [jnp.where(merged, system, 0.0) for system in systems]
        if inverses is None:
            inverses = [eye - piece for piece in pieces]
        else:
            firsts = [low_dot(inverse, piece) for inverse, piece in zip(inverses, pieces)]
            inverses = [
                inverse - low_dot(first, inverse) for first, inverse in zip(firsts, inverses)
            ]
        width *= 2
    return inverses


def chain_terms(parts, spike_pair, spike_rows, queries):
    unit, removal, logdecay, keys, values = parts
    size = keys.shape[0]
    row = lax.broadcasted_iota(jnp.int32, (size, size), 0)
    col = lax.broadcasted_iota(jnp.int32, (size, size), 1)
    lane = lax.broadcasted_iota(jnp.int32, (1, PAIR), 1)
    first_head = lane < ATTEND_WIDTH
    upto = (row >= col).astype(jnp.float32)
    ahead = exact_dot(upto, logdecay)
    behind = ahead[-1:, :] - ahead + logdecay
    if spike_pair is not None:
        spike_ahead = exact_dot(upto, spike_pair)
        spike_behind = spike_ahead[-1:, :] - spike_ahead + spike_pair
        rows_ahead = exact_dot(spike_rows, (row <= col).astype(jnp.float32))
        rows_behind = exact_dot(spike_rows, (row >= col).astype(jnp.float32))
    out = []
    for upper in (False, True):
        totals = behind if upper else ahead
        whole = totals[:1, :] if upper else totals[-1:, :]
        inverse = jnp.exp(-totals)
        exclusive = jnp.exp(totals - logdecay)
        probed = exclusive * unit
        key_in = keys * inverse
        removal_in = removal * inverse
        left = [probed]
        tail = whole - totals
        probed_start = probed
        if spike_pair is not None:
            sp_tot = spike_behind if upper else spike_ahead
            sp_whole = sp_tot[:1, :] if upper else sp_tot[-1:, :]
            sp_row = rows_behind if upper else rows_ahead
            tail = tail + sp_whole - sp_tot
            whole = whole + sp_whole
            probed_start = unit * jnp.exp(totals - logdecay + sp_tot - spike_pair)
        tail = jnp.exp(tail)
        if queries is not None:
            weighted = jnp.exp(totals) * queries
            left.append(weighted)
            weighted_start = weighted
            if spike_pair is not None:
                weighted_start = queries * jnp.exp(totals + sp_tot)
        else:
            weighted_start = None
        strict = (row < col) if upper else (row > col)
        reach = (row <= col) if upper else (row >= col)
        right = jnp.concatenate([removal_in, key_in], axis=0)
        left = jnp.concatenate(left, axis=0)
        heads = []
        for number in range(2):
            own = first_head if number == 0 else jnp.logical_not(first_head)
            scores = low_dot_nt(jnp.where(own, left, 0.0), right)
            cols = slice(number * ATTEND_WIDTH, number * ATTEND_WIDTH + 1)
            if spike_pair is not None:
                shift = sp_tot[:, cols] - sp_row[number : number + 1, :]
                strict_fade = jnp.exp(jnp.minimum(shift - spike_pair[:, cols], 0.0))
                reach_fade = jnp.exp(jnp.minimum(shift, 0.0))
            else:
                strict_fade = reach_fade = 1.0
            system = jnp.where(strict, scores[:size, :size] * strict_fade, 0.0)
            inflow = jnp.where(strict, scores[:size, size:] * strict_fade, 0.0)
            if queries is not None:
                read_back = jnp.where(reach, scores[size:, :size] * reach_fade, 0.0)
                read_in = jnp.where(reach, scores[size:, size:] * reach_fade, 0.0)
            else:
                read_back = read_in = None
            heads.append((system, inflow, read_back, read_in))
        out.append(
            dict(
                heads=heads,
                probed_start=probed_start,
                weighted_start=weighted_start,
                keys_out=keys * tail,
                removal_out=removal * tail,
                final=jnp.exp(whole),
            )
        )
    return out


def pick(first_head, pair):
    return jnp.where(first_head, pair[0], pair[1])


def folded(block):
    kept = jnp.where(head_mask(PAIR), block, 0.0)
    return kept[:ATTEND_WIDTH] + kept[ATTEND_WIDTH:]


def unfolded(pair):
    return jnp.where(head_mask(PAIR), jnp.concatenate([pair, pair], axis=0), 0.0)


def chain_kernel(
    query_ref,
    key_ref,
    value_ref,
    low_ref,
    ctx_key_ref,
    ctx_value_ref,
    ctx_low_ref,
    raise_fading_ref,
    raise_step_ref,
    fading_ref,
    spike_ref,
    spike_row_ref,
    maps_ref,
    ctx_ref,
    reading_ref,
    inside_ref,
):
    lane = lax.broadcasted_iota(jnp.int32, (1, PAIR), 1)
    first_head = lane < ATTEND_WIDTH
    shared = (raise_fading_ref[...], raise_step_ref[...], fading_ref[...])
    keys = key_ref[...].astype(jnp.float32)
    values = value_ref[...].astype(jnp.float32)
    parts = token_features(keys, low_ref[...], *shared) + (keys, values)
    latent = chain_terms(
        parts, -spike_ref[...], -spike_row_ref[0], query_ref[...].astype(jnp.float32)
    )
    ctx_keys = ctx_key_ref[...].astype(jnp.float32)
    ctx_values = ctx_value_ref[...].astype(jnp.float32)
    ctx_parts = token_features(ctx_keys, ctx_low_ref[...], *shared) + (ctx_keys, ctx_values)
    context = chain_terms(ctx_parts, None, None, None)
    inverses = block_inverses([head[0] for terms in latent for head in terms["heads"]], None)
    ctx_inverses = block_inverses([head[0] for terms in context for head in terms["heads"]], None)
    inside = None
    for way in range(2):
        terms = latent[way]
        inverse = inverses[2 * way : 2 * way + 2]
        flow = pick(first_head, [low_dot(head[1], values) for head in terms["heads"]])
        joined = jnp.concatenate([terms["probed_start"], flow], axis=1)
        solved = [low_dot(one, joined) for one in inverse]
        on_state = pick(first_head, [one[:, :PAIR] for one in solved])
        alone = pick(first_head, [one[:, PAIR:] for one in solved])
        both = jnp.concatenate([on_state, alone], axis=1)
        back = [low_dot(head[2], both) for head in terms["heads"]]
        read = pick(first_head, [low_dot(head[3], values) for head in terms["heads"]])
        reading_ref[way] = (
            terms["weighted_start"] - pick(first_head, [one[:, :PAIR] for one in back])
        ).astype(reading_ref.dtype)
        part = read - pick(first_head, [one[:, PAIR:] for one in back])
        inside = part if inside is None else inside + part
        crossed = low_dot_tn(both, terms["removal_out"])
        eye = lax.broadcasted_iota(jnp.int32, (PAIR, PAIR), 0) == lax.broadcasted_iota(
            jnp.int32, (PAIR, PAIR), 1
        )
        factor = jnp.where(eye, terms["final"], 0.0) - crossed[:PAIR]
        offset = low_dot_tn(values, terms["keys_out"]) - crossed[PAIR:]
        maps_ref[way, 0, 0] = folded(factor).astype(maps_ref.dtype)
        maps_ref[way, 0, 1] = folded(offset).astype(maps_ref.dtype)
        ctx_terms = context[way]
        ctx_inverse = ctx_inverses[2 * way : 2 * way + 2]
        flow = pick(first_head, [low_dot(head[1], ctx_values) for head in ctx_terms["heads"]])
        alone = pick(first_head, [low_dot(one, flow) for one in ctx_inverse])
        ctx_ref[way, 0] = folded(
            low_dot_tn(ctx_values, ctx_terms["keys_out"])
            - low_dot_tn(alone, ctx_terms["removal_out"])
        )
    inside_ref[...] = inside


def chain_call(
    query, key, value, low, ctx_key, ctx_value, ctx_low, raise_fading, raise_step, fading, spike
):
    rows, width = key.shape
    ctx_rows = ctx_key.shape[0]
    pairs = width // PAIR
    rank = low.shape[1]
    spike_pair = jnp.repeat(spike, ATTEND_WIDTH, axis=1)
    spike_rows = jnp.transpose(spike).reshape(pairs, 2, rows)
    columns = lambda height: pl.BlockSpec((height, PAIR), lambda i: (0, i))
    entire = lambda height: pl.BlockSpec((height, rank), lambda i: (0, 0))
    return pl.pallas_call(
        chain_kernel,
        grid=(pairs,),
        in_specs=[
            columns(rows),
            columns(rows),
            columns(rows),
            entire(rows),
            columns(ctx_rows),
            columns(ctx_rows),
            entire(ctx_rows),
            columns(rank),
            columns(rank),
            columns(1),
            columns(rows),
            pl.BlockSpec((1, 2, rows), lambda i: (i, 0, 0)),
        ],
        out_specs=[
            pl.BlockSpec((2, 1, 2, ATTEND_WIDTH, PAIR), lambda i: (0, i, 0, 0, 0)),
            pl.BlockSpec((2, 1, ATTEND_WIDTH, PAIR), lambda i: (0, i, 0, 0)),
            pl.BlockSpec((2, rows, PAIR), lambda i: (0, 0, i)),
            columns(rows),
        ],
        out_shape=[
            jax.ShapeDtypeStruct((2, pairs, 2, ATTEND_WIDTH, PAIR), jnp.bfloat16),
            jax.ShapeDtypeStruct((2, pairs, ATTEND_WIDTH, PAIR), jnp.float32),
            jax.ShapeDtypeStruct((2, rows, width), jnp.bfloat16),
            jax.ShapeDtypeStruct((rows, width), jnp.float32),
        ],
        compiler_params=pltpu.CompilerParams(dimension_semantics=("arbitrary",)),
        cost_estimate=pl.CostEstimate(
            flops=pairs * 8 * 17 * 2 * PAIR**3, bytes_accessed=4 << 20, transcendentals=0
        ),
    )(
        query,
        key,
        value,
        low,
        ctx_key,
        ctx_value,
        ctx_low,
        raise_fading,
        raise_step,
        fading.reshape(1, width),
        spike_pair,
        spike_rows,
    )


def read_kernel(own_ref, maps_ref, ctx_ref, reading_ref, inside_ref, gains_ref, normed_ref):
    shards = maps_ref.shape[0]
    pairs = maps_ref.shape[2]
    own = own_ref[0]
    same_head = head_mask(PAIR).astype(jnp.float32) * (1.0 / ATTEND_WIDTH)
    states = [
        [unfolded(ctx_ref[way, pair]) for pair in range(pairs)] for way in range(2)
    ]
    for number in range(shards - 1):
        for way in range(2):
            source = number if way == 0 else shards - 1 - number
            passed = (number < own) if way == 0 else (source > own)
            for pair in range(pairs):
                factor = unfolded(maps_ref[source, way, pair, 0].astype(jnp.float32))
                offset = unfolded(maps_ref[source, way, pair, 1].astype(jnp.float32))
                state = states[way][pair]
                states[way][pair] = jnp.where(passed, low_dot(state, factor) + offset, state)
    for pair in range(pairs):
        cols = slice(pair * PAIR, (pair + 1) * PAIR)
        combined = (
            inside_ref[:, cols]
            + low_dot_nt(reading_ref[0, :, cols], states[0][pair])
            + low_dot_nt(reading_ref[1, :, cols], states[1][pair])
        )
        centred = combined - exact_dot(combined, same_head)
        spread = exact_dot(centred * centred, same_head)
        normed = centred * lax.rsqrt(spread + EPS_HEAD) * gains_ref[:, cols]
        normed_ref[:, cols] = normed.astype(normed_ref.dtype)


def read_call(own, maps, ctx, reading, inside, gains):
    rows, width = inside.shape
    vmem = pl.BlockSpec(memory_space=pltpu.VMEM)
    return pl.pallas_call(
        read_kernel,
        in_specs=[pl.BlockSpec(memory_space=pltpu.SMEM)] + [vmem] * 5,
        out_specs=vmem,
        out_shape=jax.ShapeDtypeStruct((rows, width), jnp.bfloat16),
        cost_estimate=pl.CostEstimate(
            flops=8 * 4 * 2 * PAIR**3, bytes_accessed=4 << 20, transcendentals=0
        ),
    )(own.reshape(1), maps, ctx, reading, inside, gains.reshape(1, width))


def body(
    hidden_items,
    sample_cond,
    prompt_items,
    prompt_cond,
    adjust_shifting,
    adjust_stretch,
    skip_valve,
    receiver_matrix,
    address_matrix,
    payload_matrix,
    joint_lower_projector,
    fading_raise_matrix,
    step_raise_matrix,
    feature_fading,
    spike_logfade,
    group_standard_factor,
    emit_matrix,
):
    span_rows = adjust_shifting.shape[0]
    conditions = jnp.stack([sample_cond, prompt_cond])
    activated = jax.nn.silu(conditions.astype(jnp.float32)).astype(jnp.bfloat16)
    own_cols = lax.dynamic_slice_in_dim(activated, lax.axis_index("sp") * span_rows, span_rows, 1)
    partial = jnp.concatenate(
        [
            product(own_cols, adjust_shifting),
            product(own_cols, adjust_stretch),
            product(own_cols[:1], skip_valve),
        ],
        axis=0,
    )
    gathered = lax.all_gather(partial, ("sp", "tp"), axis=0, tiled=False)
    sp_count, tp_count = lax.axis_size("sp"), lax.axis_size("tp")
    gathered = gathered.reshape((sp_count, tp_count) + partial.shape)
    vectors = jnp.sum(gathered, axis=0)
    vectors = jnp.transpose(vectors, (1, 0, 2)).reshape(partial.shape[0], -1)
    shifts, scales, gates = vectors[:2], vectors[2:4], vectors[4:]
    down_weight = lax.all_gather(joint_lower_projector, "sp", axis=0, tiled=True)
    out_weight = lax.all_gather(emit_matrix, "sp", axis=1, tiled=True)
    u_rows = modulate(hidden_items, shifts[0], scales[0])
    features = lax.all_gather(u_rows, "tp", axis=0, tiled=True)
    ctx_mod = modulate(prompt_items, shifts[1], scales[1])
    rows = features.shape[0]
    both = jnp.concatenate([features, ctx_mod], axis=0)
    key = stored(product(both, address_matrix))
    value = stored(product(both, payload_matrix))
    low = stored(product(both, down_weight))
    query = stored(product(features, receiver_matrix))
    head_cols = key.shape[1]
    ctx_joined = jnp.concatenate([key[rows:], value[rows:], low[rows:]], axis=1)
    ctx_joined = lax.all_gather(ctx_joined, "sp", axis=0, tiled=True)
    maps, ctx_state, reading, inside = chain_call(
        query,
        key[:rows],
        value[:rows],
        low[:rows],
        ctx_joined[:, :head_cols],
        ctx_joined[:, head_cols : 2 * head_cols],
        ctx_joined[:, 2 * head_cols :],
        fading_raise_matrix,
        step_raise_matrix,
        feature_fading,
        spike_logfade,
    )
    every = lax.all_gather(maps, "sp", axis=0, tiled=False)
    normed = read_call(
        lax.axis_index("sp"), every, ctx_state, reading, inside, group_standard_factor
    )
    mixed_sum = lax.psum_scatter(
        product(normed, out_weight).astype(jnp.bfloat16), "tp", scatter_dimension=0, tiled=True
    ).astype(jnp.float32)
    return (hidden_items.astype(jnp.float32) + gates[0] * mixed_sum).astype(jnp.bfloat16)


def solution(mesh):
    placed = (
        P(("grp", "sp", "tp"), None),
        P("grp"),
        P(("grp", "sp"), None),
        P(),
        P("sp", "tp"),
        P("sp", "tp"),
        P("sp", "tp"),
        P(None, "tp"),
        P(None, "tp"),
        P(None, "tp"),
        P("sp", None),
        P(None, "tp"),
        P(None, "tp"),
        P("tp"),
        P(("grp", "sp"), "tp"),
        P("tp"),
        P("tp", "sp"),
    )
    return jax.shard_map(
        body, mesh=mesh, in_specs=placed, out_specs=P(("grp", "sp", "tp"), None), check_vma=False
    )
```

time: 881 us -> 251 us (0.28)
  other arithmetic: 511 us -> 4.52 us
  matrix products: 110 us -> 16.6 us
  waiting for transfers between devices: 34.4 us -> 127 us
  local copies, waits for them, and re-layouts: 85.3 us -> 6.24 us
  blocking collectives: 111 us -> 55.7 us
  Pallas kernels: 0 us -> 27.5 us
    another operation x28 -> x0, other arithmetic: 487 us -> none  [the longest x18 479 us: sub_block(): jax.scipy.linalg.solve_triangular(system, right_side, lower=True, unit_di...]
    all_gather x3, waiting for transfers between devices: 14.7 us -> 102 us  [the longest x1 77.7 us: body(): out_weight = lax.all_gather(emit_matrix, 'sp', axis=1, tiled=True)]
    dot_general x54 -> x0, matrix products: 74.9 us -> none  [batch_dot(): return jnp.matmul(left, right, precision=EXACT_MODE)]
    dynamic_slice x26 -> x0, local copies, waits for them, and re-layouts: 34.8 us -> none  [the longest x22 32.4 us: run_chain(): lax.scan(advance, carried, tuple((to_blocks(tensor) for tensor in inputs)))]
    all_gather x6 -> x2, blocking collectives: 72.6 us -> 38.6 us  [the longest x1 24.6 us: body(): gathered = lax.all_gather(partial, ('sp', 'tp'), axis=0, tiled=False)]
    pallas_call x0 -> x2, Pallas kernels: none -> 27.5 us  [the longest x1 23.5 us: chain_call(): pl.pallas_call(chain_kernel, grid=(pairs,), in_specs=[columns(rows), colu...]
    another operation x23 -> x0, local copies, waits for them, and re-layouts: 24.4 us -> none  [the longest x22 24.3 us: both_ways(): return jnp.stack([tensor, jnp.flip(tensor, axis=1)])]
    psum x1 -> x0, blocking collectives: 20.3 us -> none  [body(): summed = lax.psum((part_shift, part_scale, part_gate), 'sp')]
  transfers between devices with their start and end apart: 4 -> 4, of which waited for: 2 -> 3; matrix products, arithmetic and copies ran while one was open for 54% -> 1% of each run, Pallas kernels for 0% -> 2%
where the time goes in v1:
time: 251 us
  waiting for transfers between devices  127 us (51%)
  blocking collectives  55.7 us (22%)
  Pallas kernels  27.5 us (11%)
  matrix products  16.6 us (7%)
  between operations  13.3 us (5%)
  local copies, waits for them, and re-layouts  6.24 us (2%)
  other arithmetic  4.52 us (2%)
    all_gather x1, waiting for transfers between devices, body(): out_weight = lax.all_gather(emit_matrix, 'sp', axis=1, tiled=True)  77.7 us
    all_gather x1, waiting for transfers between devices, body(): every = lax.all_gather(maps, 'sp', axis=0, tiled=False)  24.7 us
    all_gather x1, blocking collectives, body(): gathered = lax.all_gather(partial, ('sp', 'tp'), axis=0, tiled=False)  24.6 us
    pallas_call x1, Pallas kernels, chain_call(): pl.pallas_call(chain_kernel, grid=(pairs,), in_specs=[columns(rows), colu...  23.5 us
    reduce_scatter x1, waiting for transfers between devices, body(): lax.psum_scatter(product(normed, out_weight).astype(jnp.bfloat16), 'tp',...  23.4 us
    all_gather x1, blocking collectives, body(): lax.all_gather(joint_lower_projector, 'sp', axis=0, tiled=True)  17.1 us
    dot_general x8, matrix products, product(): return jnp.dot(left, right, preferred_element_type=jnp.float32)  16.6 us
    all_gather x1, blocking collectives, body(): ctx_joined = lax.all_gather(ctx_joined, 'sp', axis=0, tiled=True)  14 us
  transfers between devices with their start and end apart: 4, of which 3 were waited for; matrix products, arithmetic and copies ran while one was open for 1% of the time, Pallas kernels for 2%

profile of v1, /device:TPU:0, one launch (start us, length us, event | category | flops | bytes accessed | tf_op | source)
XLA Modules:
  0.0 250.5 jit_solution(8162634746813809551)
XLA Ops:
  6.5 0.0 all-gather.7.cloned.1.call-start
  6.5 0.9 stack.10
  7.4 0.7 stack.9
  8.1 0.0 copy-start.3
  8.2 0.0 copy-done
  8.2 0.4 fusion.20
  8.6 2.1 fusion.21
  10.7 0.0 copy-start.6
  10.7 0.4 fusion.14
  11.1 24.6 %all-gather.2 = f32[16,5,1024]{2,1,0:T(8,128)S(1)} all-gather(f32[1,5,1024]{2,1,0:T(8,128)S(1)} %maximum_bitcast_fusion), channel_id=2, replica_groups=mesh['grp'=2,'sp'=4,'tp'=4] {'sp','tp'}, dimensions={0}, use_global_device_ids=true | all-gather | bytes 348160 | tf_op jit(solution)/shard_map/all_gather | solution.py:397
  35.8 0.1 fusion.19
  35.9 0.2 convert_reduce_fusion
  36.0 0.3 fusion.4
  36.3 0.9 fusion.7
  37.2 0.0 all-gather.7.cloned.1.call-update
  37.2 0.0 all-gather.11.cloned.1.call-start
  37.3 0.2 convert_reduce_fusion.1
  37.5 0.8 copy.26.spike_ref
  38.3 0.3 fusion.8
  38.5 0.0 copy-done.6
  38.5 17.1 %all_gather.27 = bf16[4096,64]{0,1:T(8,128)(2,1)} all-gather(bf16[1024,64]{0,1:T(8,128)(2,1)S(1)} %copy-done.6), channel_id=1, replica_groups=mesh['grp'=2,'sp'=4,'tp'=4] {'sp'}, dimensions={0}, use_global_device_ids=true | all-gather | bytes 655360 | tf_op jit(solution)/shard_map/all_gather | solution.py:403
  55.6 0.9 fusion.11
  56.5 2.1 convolution_convert_fusion.4
  58.6 0.1 copy.28
  58.7 0.0 copy-start.5
  58.7 0.0 copy-start.8
  58.7 3.3 %convolution_convert_fusion.1 = bf16[160,512]{1,0:T(8,128)(2,1)S(1)} fusion(bf16[4096,512]{1,0:T(8,128)(2,1)} %param.26, bf16[32,4096]{1,0:T(8,128)(2,1)} %fusion.11, bf16[128,4096]{1,0:T(8,128)(2,1)S(1)} %copy-done.4), kind=kOutput, calls=%fused_computation.2 | convolution fusion | flops 673792000 | bytes 5668864 | tf_op jit(solution)/shard_map/dot_general | solution.py:26
  62.0 0.3 copy-done.8
  62.3 0.9 convolution_convert_fusion.2
  63.2 14.0 %all_gather.28 = bf16[128,1088]{1,0:T(8,128)(2,1)S(1)} all-gather(bf16[32,1088]{1,0:T(8,128)(2,1)S(1)} %pad_maximum_fusion.4), channel_id=1, replica_groups=mesh['grp'=2,'sp'=4,'tp'=4] {'sp'}, dimensions={0}, use_global_device_ids=true | all-gather | bytes 348160 | tf_op jit(solution)/shard_map/all_gather | solution.py:416
  77.2 0.7 fusion.18
  77.9 0.6 slice.87.ctx_low_ref
  78.5 0.7 slice.80.value_ref
  79.2 0.7 slice.79.key_ref
  79.9 0.7 copy.27.low_ref
  80.6 3.6 %convolution_convert_fusion.3.query_ref = bf16[128,512]{1,0:T(8,128)(2,1)} fusion(bf16[128,4096]{1,0:T(8,128)(2,1)S(1)} %copy-done.4, bf16[4096,512]{1,0:T(8,128)(2,1)} %param.24), kind=kOutput, calls=%fused_computation.4 | convolution fusion | flops 536936448 | bytes 5373952 | tf_op jit(solution)/shard_map/dot_general | solution.py:26
  84.1 23.5 %shard_map.163 = (bf16[2,4,2,64,128]{4,3,2,1,0:T(8,128)(2,1)}, f32[2,4,64,128]{3,2,1,0:T(8,128)}, bf16[2,128,512]{2,1,0:T(8,128)(2,1)}, f32[128,512]{1,0:T(8,128)}) custom-call(bf16[128,512]{1,0:T(8,128)(2,1)} %convolution_convert_fusion.3.query_ref, bf16[128,512]{1,0:T(8,128)(2,1)} %slice.79.key_ref, bf16[128,512]{1,0:T(8,128)(2,1)} %slice.80.value_ref, ...), custom_call_target="tpu_custom_call" | custom-call | flops 2281701376 | bytes 4194304 | tf_op jit(solution)/shard_map/pallas_call | solution.py:273
  107.6 0.0 all-gather.11.cloned.1.call-update
  107.7 0.0 all-gather.9.cloned.1.call-start
  107.7 0.7 all-gather.9.cloned.1.call-update
  108.4 0.0 reduce-scatter.2.cloned.1.call-start
  108.4 24.7 %all-gather.11.cloned.1.call-done = bf16[8,4,2,64,128]{4,3,2,1,0:T(8,128)(2,1)} async-done(((bf16[2,4,2,64,128]{4,3,2,1,0:T(8,128)(2,1)}), bf16[8,4,2,64,128]{4,3,2,1,0:T(8,128)(2,1)}) %all-gather.11.cloned.1.call-update) | async-done | bytes 1048592 | tf_op jit(solution)/shard_map/all_gather | solution.py:430
  133.2 4.0 %shard_map.164 = bf16[128,512]{1,0:T(8,128)(2,1)} custom-call(s32[1]{0:T(128)} %bitcast.5.own_ref, bf16[4,2,4,2,64,128]{5,4,3,2,1,0:T(8,128)(2,1)} %bitcast.34, f32[2,4,64,128]{3,2,1,0:T(8,128)} %get-tuple-element.10.ctx_ref, bf16[2,128,512]{2,1,0:T(8,128)(2,1)} %get-tuple-element.11.reading_ref, f32[128,512]{1,0:T(8,128)} %get-tuple-element.12.inside_ref, ...), custom_call_target="tpu_custom_call" | custom-call | flops 134217728 | bytes 4194304 | tf_op jit(solution)/shard_map/pallas_call | solution.py:355
  137.2 77.7 %all-gather.9.cloned.1.call-done = bf16[512,4096]{1,0:T(8,128)(2,1)} async-done(((bf16[512,1024]{1,0:T(8,128)(2,1)}), bf16[512,4096]{1,0:T(8,128)(2,1)}) %all-gather.9.cloned.1.call-update) | async-done | bytes 4194320 | tf_op jit(solution)/shard_map/all_gather | solution.py:404
  214.9 4.0 %convolution_convert_fusion = bf16[128,4096]{1,0:T(8,128)(2,1)} fusion(bf16[128,512]{1,0:T(8,128)(2,1)} %shard_map.164, bf16[512,4096]{1,0:T(8,128)(2,1)} %all-gather.9.cloned.1.call-done), kind=kOutput, calls=%fused_computation | convolution fusion | flops 537395200 | bytes 5373952 | tf_op jit(solution)/shard_map/dot_general | solution.py:26
  218.8 0.0 reduce-scatter.2.cloned.1.call-update
  218.9 23.4 %reduce-scatter.2.cloned.1.call-done = bf16[32,4096]{1,0:T(8,128)(2,1)} async-done(((bf16[128,4096]{1,0:T(8,128)(2,1)}), bf16[32,4096]{1,0:T(8,128)(2,1)}) %reduce-scatter.2.cloned.1.call-update) | async-done | bytes 262160 | tf_op jit(solution)/shard_map/reduce_scatter | solution.py:434
  242.3 1.7 fusion.12
  (26 shorter events, 0.2 us)
Async XLA Ops:
  6.5 1.7 copy-start
  6.5 49.9 %all-gather.7.cloned.1.call-start = ((), (), s32[]{:S(2)}) async-start(), calls=%async_computation.1 | async-start | bytes 1310720 | tf_op jit(solution)/shard_map/all_gather | solution.py:406
  8.1 2.6 %copy-start.3 = (bf16[1024,1024]{1,0:T(8,128)(2,1)S(1)}, bf16[1024,1024]{1,0:T(8,128)(2,1)}, u32[]{:S(2)}) copy-start(bf16[1024,1024]{1,0:T(8,128)(2,1)} %param.23) | copy-start | bytes 6291460
  8.6 27.3 %copy-start.1 = (bf16[32,4096]{1,0:T(8,128)(2,1)S(1)}, bf16[32,4096]{1,0:T(8,128)(2,1)}, u32[]{:S(2)}) copy-start(bf16[32,4096]{1,0:T(8,128)(2,1)} %param.17) | copy-start | bytes 786436
  10.7 26.5 %copy-start.2 = (bf16[32,4096]{1,0:T(8,128)(2,1)S(1)}, bf16[32,4096]{1,0:T(8,128)(2,1)}, u32[]{:S(2)}) copy-start(bf16[32,4096]{1,0:T(8,128)(2,1)} %param.19) | copy-start | bytes 786436
  10.7 26.7 %copy-start.7 = (f32[128,8]{0,1:T(8,128)S(1)}, f32[128,8]{0,1:T(8,128)}, u32[]{:S(2)}) copy-start(f32[128,8]{0,1:T(8,128)} %param.31) | copy-start | bytes 12292
  10.7 27.8 %copy-start.6 = (bf16[1024,64]{0,1:T(8,128)(2,1)S(1)}, bf16[1024,64]{0,1:T(8,128)(2,1)}, u32[]{:S(2)}) copy-start(bf16[1024,64]{0,1:T(8,128)(2,1)} %param.27) | copy-start | bytes 393220
  37.2 96.0 %all-gather.11.cloned.1.call-start = ((), (), s32[]{:S(2)}) async-start(), calls=%async_computation.4 | async-start | bytes 1310720 | tf_op jit(solution)/shard_map/all_gather | solution.py:430
  56.5 2.2 copy-start.4
  58.7 3.3 %copy-start.5 = (bf16[32,4096]{1,0:T(8,128)(2,1)S(1)}, bf16[32,4096]{1,0:T(8,128)(2,1)}, u32[]{:S(2)}) copy-start(bf16[32,4096]{1,0:T(8,128)(2,1)} %fusion.11) | copy-start | bytes 786436
  58.7 3.6 %copy-start.8 = (bf16[4096,512]{1,0:T(8,128)(2,1)S(1)}, bf16[4096,512]{1,0:T(8,128)(2,1)}, u32[]{:S(2)}) copy-start(bf16[4096,512]{1,0:T(8,128)(2,1)} %param.25) | copy-start | bytes 12582916
  107.7 107.2 %all-gather.9.cloned.1.call-start = ((), (), s32[]{:S(2)}) async-start(), calls=%async_computation.2 | async-start | bytes 5242880 | tf_op jit(solution)/shard_map/all_gather | solution.py:404
  108.4 133.9 %reduce-scatter.2.cloned.1.call-start = ((), (), s32[]{:S(2)}) async-start(), calls=%async_computation.3 | async-start | bytes 1310720 | tf_op jit(solution)/shard_map/reduce_scatter | solution.py:434
Sparse Core Ops, SparseCore 0:
  37.3 13.9 all-gather.6
  107.8 25.3 all-gather.10
  134.7 80.1 all-gather.8
  219.0 23.2 reduce-scatter.1

commit v2 on v1

--- a/solution.py
+++ b/solution.py
@@ -219,7 +219,7 @@
     )
     ctx_keys = ctx_key_ref[...].astype(jnp.float32)
     ctx_values = ctx_value_ref[...].astype(jnp.float32)
-    ctx_parts = token_features(ctx_keys, ctx_low_ref[...], *shared) + (ctx_keys, ctx_values)
+    ctx_parts = token_features(ctx_keys, ctx_low_ref[:, : low_ref.shape[1]], *shared) + (ctx_keys, ctx_values)
     context = chain_terms(ctx_parts, None, None, None)
     inverses = block_inverses([head[0] for terms in latent for head in terms["heads"]], None)
     ctx_inverses = block_inverses([head[0] for terms in context for head in terms["heads"]], None)
@@ -260,10 +260,10 @@
 
 
 def chain_call(
-    query, key, value, low, ctx_key, ctx_value, ctx_low, raise_fading, raise_step, fading, spike
+    query, key, value, low, ctx_all, raise_fading, raise_step, fading, spike
 ):
     rows, width = key.shape
-    ctx_rows = ctx_key.shape[0]
+    ctx_rows = ctx_all.shape[0]
     pairs = width // PAIR
     rank = low.shape[1]
     spike_pair = jnp.repeat(spike, ATTEND_WIDTH, axis=1)
@@ -279,8 +279,8 @@
             columns(rows),
             entire(rows),
             columns(ctx_rows),
-            columns(ctx_rows),
-            entire(ctx_rows),
+            pl.BlockSpec((ctx_rows, PAIR), lambda i: (0, pairs + i)),
+            pl.BlockSpec((ctx_rows, PAIR), lambda i: (0, 2 * pairs)),
             columns(rank),
             columns(rank),
             columns(1),
@@ -308,9 +308,9 @@
         key,
         value,
         low,
-        ctx_key,
-        ctx_value,
-        ctx_low,
+        ctx_all,
+        ctx_all,
+        ctx_all,
         raise_fading,
         raise_step,
         fading.reshape(1, width),
@@ -319,48 +319,424 @@
     )
 
 
-def read_kernel(own_ref, maps_ref, ctx_ref, reading_ref, inside_ref, gains_ref, normed_ref):
-    shards = maps_ref.shape[0]
-    pairs = maps_ref.shape[2]
-    own = own_ref[0]
+MESH_ID = pl.DeviceIdType.MESH
+
+
+def remote(source, target, send_sem, recv_sem, device):
+    return pltpu.make_async_remote_copy(
+        src_ref=source,
+        dst_ref=target,
+        send_sem=send_sem,
+        recv_sem=recv_sem,
+        device_id=device,
+        device_id_type=MESH_ID,
+    )
+
+
+def greet(devices):
+    barrier = pltpu.get_barrier_semaphore()
+    for device in devices:
+        pl.semaphore_signal(barrier, inc=1, device_id=device, device_id_type=MESH_ID)
+    pl.semaphore_wait(barrier, len(devices))
+
+
+def others(axis, count):
+    own = lax.axis_index(axis)
+    return [{axis: lax.rem(own + step, count)} for step in range(1, count)]
+
+
+def front_kernel(
+    sp_count,
+    tp_count,
+    active_ref,
+    shift_ref,
+    scale_ref,
+    valve_ref,
+    hidden_ref,
+    prompt_ref,
+    down_ref,
+    rows_ref,
+    ctx_ref,
+    gates_ref,
+    down_all_ref,
+    partial_ref,
+    vector_ref,
+    down_send,
+    down_recv,
+    part_send,
+    part_recv,
+    vec_send,
+    vec_recv,
+    row_send,
+    row_recv,
+    mate_send,
+    mate_recv,
+):
+    sp_own, tp_own = lax.axis_index("sp"), lax.axis_index("tp")
+    sp_peers, tp_peers = others("sp", sp_count), others("tp", tp_count)
+    greet(sp_peers + tp_peers)
+    local = jnp.dot(active_ref[0], shift_ref[...], preferred_element_type=jnp.float32)
+    local += jnp.dot(active_ref[1], scale_ref[...], preferred_element_type=jnp.float32)
+    local += jnp.dot(active_ref[2], valve_ref[...], preferred_element_type=jnp.float32)
+    partial_ref[0] = local[:8]
+    part_copies = [
+        remote(
+            partial_ref.at[0],
+            partial_ref.at[step + 1],
+            part_send.at[step],
+            part_recv.at[step],
+            peer,
+        )
+        for step, peer in enumerate(sp_peers)
+    ]
+    for copy in part_copies:
+        copy.start()
+    down_copies = [
+        remote(
+            down_ref, down_all_ref.at[sp_own], down_send.at[step], down_recv.at[step], peer
+        )
+        for step, peer in enumerate(sp_peers)
+    ]
+    for copy in down_copies:
+        copy.start()
+    down_all_ref[sp_own] = down_ref[...]
+
+    def statistics(ref):
+        values = ref[...].astype(jnp.float32)
+        centre = jnp.mean(values, -1, keepdims=True)
+        spread = jnp.mean(jnp.square(values - centre), -1, keepdims=True)
+        return centre, lax.rsqrt(spread + EPS_ROW)
+
+    hidden_stats, prompt_stats = statistics(hidden_ref), statistics(prompt_ref)
+    for copy in part_copies:
+        copy.wait_recv()
+    vector_ref[tp_own] = jnp.sum(partial_ref[...], axis=0)
+    vec_copies = [
+        remote(
+            vector_ref.at[tp_own],
+            vector_ref.at[tp_own],
+            vec_send.at[step],
+            vec_recv.at[step],
+            peer,
+        )
+        for step, peer in enumerate(tp_peers)
+    ]
+    for copy in vec_copies:
+        copy.start()
+    for copy in vec_copies:
+        copy.wait_recv()
+    span = vector_ref.shape[2]
+
+    def modulated(ref, stats, which, number):
+        vector = vector_ref[number]
+        values = ref[:, number * span : (number + 1) * span].astype(jnp.float32)
+        normed = (values - stats[0]) * stats[1]
+        changed = normed * (1.0 + vector[2 + which : 3 + which]) + vector[which : which + 1]
+        return changed.astype(jnp.bfloat16)
+
+    for number in range(tp_count):
+        cols = slice(number * span, (number + 1) * span)
+        rows_ref[tp_own, :, cols] = modulated(hidden_ref, hidden_stats, 0, number)
+    chips = tp_count // 2
+    chip, core = tp_own // 2, lax.rem(tp_own, 2)
+    mate = {"tp": chip * 2 + 1 - core}
+    height = rows_ref.shape[1]
+    halves = 2 if height % 32 == 0 else 1
+    part = height // halves
+    spans = [pl.ds(half * part, part) for half in range(halves)]
+    chip_copies = []
+    for step in range(1, chips):
+        target = {"tp": lax.rem(chip + step, chips) * 2 + core}
+        for half, rows in enumerate(spans):
+            slot = (step - 1) * halves + half
+            block = rows_ref.at[tp_own, rows]
+            chip_copies.append(
+                remote(block, block, row_send.at[slot], row_recv.at[slot], target)
+            )
+    last = (chips - 1) * halves
+    own_block = rows_ref.at[tp_own]
+    mate_copies = [remote(own_block, own_block, mate_send.at[last], mate_recv.at[last], mate)]
+    for copy in chip_copies + mate_copies:
+        copy.start()
+    for number in range(tp_count):
+        cols = slice(number * span, (number + 1) * span)
+        ctx_ref[:, cols] = modulated(prompt_ref, prompt_stats, 1, number)
+        gates_ref[:, cols] = vector_ref[number, 4:5]
+    for step in range(1, chips):
+        source = lax.rem(chip + chips - step, chips) * 2 + core
+        for half, rows in enumerate(spans):
+            slot = (step - 1) * halves + half
+            chip_copies[slot].wait_recv()
+            block = rows_ref.at[source, rows]
+            copy = remote(block, block, mate_send.at[slot], mate_recv.at[slot], mate)
+            copy.start()
+            mate_copies.append(copy)
+    for copy in mate_copies + down_copies:
+        copy.wait_recv()
+    for copy in part_copies + down_copies + vec_copies + chip_copies + mate_copies:
+        copy.wait_send()
+
+
+VMEM_SPEC = pl.BlockSpec(memory_space=pltpu.VMEM)
+
+
+def front_call(active, shift, scale, valve, hidden, prompt, down):
+    sp_count, tp_count = lax.axis_size("sp"), lax.axis_size("tp")
+    width = hidden.shape[1]
+    dma = pltpu.SemaphoreType.DMA
+    return pl.pallas_call(
+        functools.partial(front_kernel, sp_count, tp_count),
+        in_specs=[VMEM_SPEC] * 7,
+        out_specs=[VMEM_SPEC] * 4,
+        out_shape=[
+            jax.ShapeDtypeStruct((tp_count,) + hidden.shape, jnp.bfloat16),
+            jax.ShapeDtypeStruct(prompt.shape, jnp.bfloat16),
+            jax.ShapeDtypeStruct((1, width), jnp.float32),
+            jax.ShapeDtypeStruct((sp_count,) + down.shape, jnp.bfloat16),
+        ],
+        scratch_shapes=[
+            pltpu.VMEM((sp_count, 8, shift.shape[1]), jnp.float32),
+            pltpu.VMEM((tp_count, 8, shift.shape[1]), jnp.float32),
+        ]
+        + [dma((sp_count,))] * 4
+        + [dma((tp_count,))] * 6,
+        compiler_params=pltpu.CompilerParams(collective_id=0, has_side_effects=True),
+        cost_estimate=pl.CostEstimate(
+            flops=1 << 20, bytes_accessed=60 << 20, transcendentals=0
+        ),
+    )(active, shift, scale, valve, hidden, prompt, down)
+
+
+def spread_kernel(count, own_ref, all_ref, send, recv):
+    own = lax.axis_index("sp")
+    peers = others("sp", count)
+    greet(peers)
+    copies = [
+        remote(own_ref, all_ref.at[own], send.at[step], recv.at[step], peer)
+        for step, peer in enumerate(peers)
+    ]
+    for copy in copies:
+        copy.start()
+    all_ref[own] = own_ref[...]
+    for copy in copies:
+        copy.wait()
+
+
+def spread_call(block):
+    count = lax.axis_size("sp")
+    dma = pltpu.SemaphoreType.DMA
+    return pl.pallas_call(
+        functools.partial(spread_kernel, count),
+        in_specs=[VMEM_SPEC],
+        out_specs=VMEM_SPEC,
+        out_shape=jax.ShapeDtypeStruct((count,) + block.shape, block.dtype),
+        scratch_shapes=[dma((count,)), dma((count,))],
+        compiler_params=pltpu.CompilerParams(collective_id=1, has_side_effects=True),
+        cost_estimate=pl.CostEstimate(
+            flops=1 << 20, bytes_accessed=20 << 20, transcendentals=0
+        ),
+    )(block)
+
+
+def read_kernel(
+    count,
+    maps_ref,
+    ctx_ref,
+    reading_ref,
+    inside_ref,
+    gains_ref,
+    normed_ref,
+    slots_ref,
+    state_ref,
+    send,
+    recv,
+):
+    own = lax.axis_index("sp")
+    pairs = maps_ref.shape[1]
+    greet(others("sp", count))
+
+    def transfer(way, step):
+        target = own + step if way == 0 else own - step
+        target = jnp.clip(target, 0, count - 1)
+        return remote(
+            maps_ref.at[way],
+            slots_ref.at[way, step - 1],
+            send.at[way, step - 1],
+            recv.at[way, step - 1],
+            {"sp": target},
+        )
+
+    def sending(way, step):
+        return own + step < count if way == 0 else own >= step
+
+    def receiving(way, step):
+        return own >= step if way == 0 else own + step < count
+
+    for step in range(count - 1, 0, -1):
+        for way in range(2):
+
+            @pl.when(sending(way, step))
+            def _():
+                transfer(way, step).start()
+
+    for way in range(2):
+        for pair in range(pairs):
+            state_ref[way, pair] = unfolded(ctx_ref[way, pair])
+    for step in range(count - 1, 0, -1):
+        for way in range(2):
+
+            @pl.when(receiving(way, step))
+            def _():
+                transfer(way, step).wait_recv()
+                for pair in range(pairs):
+                    factor = unfolded(slots_ref[way, step - 1, pair, 0].astype(jnp.float32))
+                    offset = unfolded(slots_ref[way, step - 1, pair, 1].astype(jnp.float32))
+                    state_ref[way, pair] = low_dot(state_ref[way, pair], factor) + offset
+
     same_head = head_mask(PAIR).astype(jnp.float32) * (1.0 / ATTEND_WIDTH)
-    states = [
-        [unfolded(ctx_ref[way, pair]) for pair in range(pairs)] for way in range(2)
-    ]
-    for number in range(shards - 1):
-        for way in range(2):
-            source = number if way == 0 else shards - 1 - number
-            passed = (number < own) if way == 0 else (source > own)
-            for pair in range(pairs):
-                factor = unfolded(maps_ref[source, way, pair, 0].astype(jnp.float32))
-                offset = unfolded(maps_ref[source, way, pair, 1].astype(jnp.float32))
-                state = states[way][pair]
-                states[way][pair] = jnp.where(passed, low_dot(state, factor) + offset, state)
     for pair in range(pairs):
         cols = slice(pair * PAIR, (pair + 1) * PAIR)
         combined = (
             inside_ref[:, cols]
-            + low_dot_nt(reading_ref[0, :, cols], states[0][pair])
-            + low_dot_nt(reading_ref[1, :, cols], states[1][pair])
+            + low_dot_nt(reading_ref[0, :, cols], state_ref[0, pair])
+            + low_dot_nt(reading_ref[1, :, cols], state_ref[1, pair])
         )
         centred = combined - exact_dot(combined, same_head)
         spread = exact_dot(centred * centred, same_head)
         normed = centred * lax.rsqrt(spread + EPS_HEAD) * gains_ref[:, cols]
         normed_ref[:, cols] = normed.astype(normed_ref.dtype)
-
-
-def read_call(own, maps, ctx, reading, inside, gains):
+    for step in range(count - 1, 0, -1):
+        for way in range(2):
+
+            @pl.when(sending(way, step))
+            def _():
+                transfer(way, step).wait_send()
+
+
+def read_call(maps, ctx, reading, inside, gains):
     rows, width = inside.shape
-    vmem = pl.BlockSpec(memory_space=pltpu.VMEM)
+    count = lax.axis_size("sp")
+    dma = pltpu.SemaphoreType.DMA
     return pl.pallas_call(
-        read_kernel,
-        in_specs=[pl.BlockSpec(memory_space=pltpu.SMEM)] + [vmem] * 5,
-        out_specs=vmem,
+        functools.partial(read_kernel, count),
+        in_specs=[VMEM_SPEC] * 5,
+        out_specs=VMEM_SPEC,
         out_shape=jax.ShapeDtypeStruct((rows, width), jnp.bfloat16),
+        scratch_shapes=[
+            pltpu.VMEM((2, count - 1) + maps.shape[1:], jnp.bfloat16),
+            pltpu.VMEM((2, maps.shape[1], PAIR, PAIR), jnp.float32),
+            dma((2, count - 1)),
+            dma((2, count - 1)),
+        ],
+        compiler_params=pltpu.CompilerParams(collective_id=2, has_side_effects=True),
         cost_estimate=pl.CostEstimate(
-            flops=8 * 4 * 2 * PAIR**3, bytes_accessed=4 << 20, transcendentals=0
+            flops=8 * 4 * 2 * PAIR**3, bytes_accessed=40 << 20, transcendentals=0
         ),
-    )(own.reshape(1), maps, ctx, reading, inside, gains.reshape(1, width))
+    )(maps, ctx, reading, inside, gains.reshape(1, width))
+
+
+def emit_kernel(
+    tp_count,
+    normed_ref,
+    weight_ref,
+    hidden_ref,
+    gates_ref,
+    out_ref,
+    product_ref,
+    mate_ref,
+    chip_ref,
+    land_ref,
+    mate_send,
+    mate_recv,
+    chip_send,
+    chip_recv,
+):
+    tp_own = lax.axis_index("tp")
+    chips = tp_count // 2
+    chip, core = tp_own // 2, lax.rem(tp_own, 2)
+    mate = {"tp": chip * 2 + 1 - core}
+    targets = [{"tp": lax.rem(chip + step, chips) * 2 + core} for step in range(1, chips)]
+    greet([mate] + targets)
+    pieces = product_ref.shape[0]
+    span = product_ref.shape[4]
+    height = out_ref.shape[0]
+    shape = (chips, 2, height, span)
+    mate_copies = []
+    for piece in range(pieces):
+        cols = slice(piece * span, (piece + 1) * span)
+        block = jnp.dot(
+            normed_ref[...], weight_ref[:, cols], preferred_element_type=jnp.float32
+        ).astype(jnp.bfloat16)
+        for place in range(chips):
+            for side in range(2):
+                first = (place * 2 + side) * height
+                product_ref[piece, side, place] = block[first : first + height]
+        copy = remote(
+            product_ref.at[piece, 1 - core],
+            mate_ref.at[piece],
+            mate_send.at[piece],
+            mate_recv.at[piece],
+            mate,
+        )
+        copy.start()
+        mate_copies.append(copy)
+    chip_copies = []
+    for piece in range(pieces):
+        mate_copies[piece].wait_recv()
+        summed = product_ref[piece, core].astype(jnp.float32) + mate_ref[piece].astype(
+            jnp.float32
+        )
+        chip_ref[piece] = summed.astype(jnp.bfloat16)
+        for step, target in enumerate(targets):
+            copy = remote(
+                chip_ref.at[piece, lax.rem(chip + step + 1, chips)],
+                land_ref.at[piece, step],
+                chip_send.at[piece, step],
+                chip_recv.at[piece, step],
+                target,
+            )
+            copy.start()
+            chip_copies.append(copy)
+    for piece in range(pieces):
+        cols = slice(piece * span, (piece + 1) * span)
+        mixed = product_ref[piece, core, chip].astype(jnp.float32) + mate_ref[
+            piece, chip
+        ].astype(jnp.float32)
+        for step in range(chips - 1):
+            chip_copies[piece * (chips - 1) + step].wait_recv()
+            mixed += land_ref[piece, step].astype(jnp.float32)
+        out_ref[:, cols] = (
+            hidden_ref[:, cols].astype(jnp.float32) + gates_ref[:, cols] * mixed
+        ).astype(out_ref.dtype)
+    for copy in mate_copies + chip_copies:
+        copy.wait_send()
+
+
+def emit_call(normed, weight, hidden, gates):
+    tp_count = lax.axis_size("tp")
+    chips = tp_count // 2
+    height, width = hidden.shape
+    pieces = math.gcd(4, width // PAIR)
+    span = width // pieces
+    dma = pltpu.SemaphoreType.DMA
+    vmem = lambda *shape: pltpu.VMEM(shape, jnp.bfloat16)
+    return pl.pallas_call(
+        functools.partial(emit_kernel, tp_count),
+        in_specs=[VMEM_SPEC] * 4,
+        out_specs=VMEM_SPEC,
+        out_shape=jax.ShapeDtypeStruct(hidden.shape, jnp.bfloat16),
+        scratch_shapes=[
+            vmem(pieces, 2, chips, height, span),
+            vmem(pieces, chips, height, span),
+            vmem(pieces, chips, height, span),
+            vmem(pieces, chips - 1, height, span),
+            dma((pieces,)),
+            dma((pieces,)),
+            dma((pieces, chips - 1)),
+            dma((pieces, chips - 1)),
+        ],
+        compiler_params=pltpu.CompilerParams(collective_id=3, has_side_effects=True),
+    )(normed, weight, hidden, gates)
 
 
 def body(
@@ -386,55 +762,51 @@
     conditions = jnp.stack([sample_cond, prompt_cond])
     activated = jax.nn.silu(conditions.astype(jnp.float32)).astype(jnp.bfloat16)
     own_cols = lax.dynamic_slice_in_dim(activated, lax.axis_index("sp") * span_rows, span_rows, 1)
-    partial = jnp.concatenate(
+    active = jnp.stack(
         [
-            product(own_cols, adjust_shifting),
-            product(own_cols, adjust_stretch),
-            product(own_cols[:1], skip_valve),
-        ],
-        axis=0,
-    )
-    gathered = lax.all_gather(partial, ("sp", "tp"), axis=0, tiled=False)
-    sp_count, tp_count = lax.axis_size("sp"), lax.axis_size("tp")
-    gathered = gathered.reshape((sp_count, tp_count) + partial.shape)
-    vectors = jnp.sum(gathered, axis=0)
-    vectors = jnp.transpose(vectors, (1, 0, 2)).reshape(partial.shape[0], -1)
-    shifts, scales, gates = vectors[:2], vectors[2:4], vectors[4:]
-    down_weight = lax.all_gather(joint_lower_projector, "sp", axis=0, tiled=True)
+            jnp.pad(own_cols, ((0, 14), (0, 0))),
+            jnp.pad(own_cols, ((2, 12), (0, 0))),
+            jnp.pad(own_cols[:1], ((4, 11), (0, 0))),
+        ]
+    )
+    half = joint_lower_projector.shape[0] // 2
+    down_own = jnp.concatenate(
+        [joint_lower_projector[:half], joint_lower_projector[half:]], axis=1
+    )
     out_weight = lax.all_gather(emit_matrix, "sp", axis=1, tiled=True)
-    u_rows = modulate(hidden_items, shifts[0], scales[0])
-    features = lax.all_gather(u_rows, "tp", axis=0, tiled=True)
-    ctx_mod = modulate(prompt_items, shifts[1], scales[1])
-    rows = features.shape[0]
-    both = jnp.concatenate([features, ctx_mod], axis=0)
-    key = stored(product(both, address_matrix))
-    value = stored(product(both, payload_matrix))
-    low = stored(product(both, down_weight))
-    query = stored(product(features, receiver_matrix))
-    head_cols = key.shape[1]
-    ctx_joined = jnp.concatenate([key[rows:], value[rows:], low[rows:]], axis=1)
-    ctx_joined = lax.all_gather(ctx_joined, "sp", axis=0, tiled=True)
+    features, ctx_mod, gates, down_all = front_call(
+        active,
+        adjust_shifting,
+        adjust_stretch,
+        skip_valve,
+        hidden_items,
+        prompt_items,
+        down_own,
+    )
+    features = features.reshape(-1, hidden_items.shape[1])
+    rank = joint_lower_projector.shape[1]
+    down_weight = jnp.stack([down_all[:, :, :rank], down_all[:, :, rank:]], axis=1)
+    down_weight = down_weight.reshape(-1, rank)
+    ctx_key = stored(product(ctx_mod, address_matrix))
+    ctx_value = stored(product(ctx_mod, payload_matrix))
+    ctx_low = stored(product(ctx_mod, down_weight))
+    ctx_joined = jnp.concatenate(
+        [ctx_key, ctx_value, jnp.pad(ctx_low, ((0, 0), (0, PAIR - rank)))], axis=1
+    )
+    ctx_all = spread_call(ctx_joined).reshape(-1, ctx_joined.shape[1])
     maps, ctx_state, reading, inside = chain_call(
-        query,
-        key[:rows],
-        value[:rows],
-        low[:rows],
-        ctx_joined[:, :head_cols],
-        ctx_joined[:, head_cols : 2 * head_cols],
-        ctx_joined[:, 2 * head_cols :],
+        stored(product(features, receiver_matrix)),
+        stored(product(features, address_matrix)),
+        stored(product(features, payload_matrix)),
+        stored(product(features, down_weight)),
+        ctx_all,
         fading_raise_matrix,
         step_raise_matrix,
         feature_fading,
         spike_logfade,
     )
-    every = lax.all_gather(maps, "sp", axis=0, tiled=False)
-    normed = read_call(
-        lax.axis_index("sp"), every, ctx_state, reading, inside, group_standard_factor
-    )
-    mixed_sum = lax.psum_scatter(
-        product(normed, out_weight).astype(jnp.bfloat16), "tp", scatter_dimension=0, tiled=True
-    ).astype(jnp.float32)
-    return (hidden_items.astype(jnp.float32) + gates[0] * mixed_sum).astype(jnp.bfloat16)
+    normed = read_call(maps, ctx_state, reading, inside, group_standard_factor)
+    return emit_call(normed, out_weight, hidden_items, gates)
 
 
 def solution(mesh):

time: 251 us -> 147 us (0.59)
  waiting for transfers between devices: 127 us -> 0.73 us
  Pallas kernels: 27.5 us -> 110 us
  blocking collectives: 55.7 us -> 0 us
  matrix products: 16.6 us -> 11.3 us
    pallas_call x1 -> x4, Pallas kernels: 4.05 us -> 86.2 us  [the longest x1 33.1 us: front_call(): pl.pallas_call(functools.partial(front_kernel, sp_count, tp_count), in_sp...]
    all_gather x1, waiting for transfers between devices: 77.7 us -> 0.02 us  [body(): out_weight = lax.all_gather(emit_matrix, 'sp', axis=1, tiled=True)]
    all_gather x3 -> x0, blocking collectives: 55.7 us -> none  [the longest x1 24.6 us: body(): gathered = lax.all_gather(partial, ('sp', 'tp'), axis=0, tiled=False)]
    all_gather x2 -> x0, waiting for transfers between devices: 24.7 us -> none  [the longest x1 24.7 us: body(): every = lax.all_gather(maps, 'sp', axis=0, tiled=False)]
    reduce_scatter x1 -> x0, waiting for transfers between devices: 23.4 us -> none  [body(): lax.psum_scatter(product(normed, out_weight).astype(jnp.bfloat16), 'tp',...]
    dot_general x8 -> x7, matrix products: 16.6 us -> 11.3 us  [product(): return jnp.dot(left, right, preferred_element_type=jnp.float32)]
    convert_element_type x3 -> x0, other arithmetic: 3.48 us -> none  [the longest x2 1.75 us: modulate(): return (normed * (1.0 + scales) + shifts).astype(jnp.bfloat16)]
  transfers between devices with their start and end apart: 4 -> 1, of which waited for: 3 -> 0; matrix products, arithmetic and copies ran while one was open for 1% -> 14% of each run, Pallas kernels for 2% -> 66%
where the time goes in v2:
time: 147 us; the launch traced here: 146 us
  Pallas kernels  110 us (75%)
  between operations  13.6 us (9%)
  matrix products  11.3 us (8%)
  local copies, waits for them, and re-layouts  8.34 us (6%)
  other arithmetic  2.37 us (2%)
    pallas_call x1, Pallas kernels, front_call(): pl.pallas_call(functools.partial(front_kernel, sp_count, tp_count), in_sp...  33.1 us
    pallas_call x1, Pallas kernels, chain_call(): pl.pallas_call(chain_kernel, grid=(pairs,), in_specs=[columns(rows), colu...  23.6 us
    pallas_call x1, Pallas kernels, spread_call(): pl.pallas_call(functools.partial(spread_kernel, count), in_specs=[VMEM_SP...  23 us
    pallas_call x1, Pallas kernels, read_call(): pl.pallas_call(functools.partial(read_kernel, count), in_specs=[VMEM_SPEC...  16.8 us
    pallas_call x1, Pallas kernels, emit_call(): pl.pallas_call(functools.partial(emit_kernel, tp_count), in_specs=[VMEM_S...  13.3 us
    dot_general x7, matrix products, product(): return jnp.dot(left, right, preferred_element_type=jnp.float32)  11.3 us
  transfers between devices with their start and end apart: 1, of which 0 were waited for; matrix products, arithmetic and copies ran while one was open for 14% of the time, Pallas kernels for 66%

profile of v2, /device:TPU:0, one launch (start us, length us, event | category | flops | bytes accessed | tf_op | source)
XLA Modules:
  0.0 146.1 jit_solution(16705495831167403476)
XLA Ops:
  6.5 0.0 all-gather.2.cloned.1.call-start
  6.5 0.7 all-gather.2.cloned.1.call-update
  7.3 0.7 stack.30
  8.0 0.7 stack.31
  8.7 0.9 fusion.3
  9.6 0.1 copy.32
  9.7 0.1 copy.33
  9.9 0.7 pad_maximum_fusion.2.active_ref
  10.6 0.8 pad_maximum_fusion.1.down_ref
  11.4 33.1 %shard_map.163 = (bf16[4,32,4096]{2,1,0:T(8,128)(2,1)}, bf16[32,4096]{1,0:T(8,128)(2,1)}, f32[1,4096]{1,0:T(1,128)}, bf16[4,512,128]{2,1,0:T(8,128)(2,1)}) custom-call(bf16[3,16,1024]{2,1,0:T(8,128)(2,1)} %pad_maximum_fusion.2.active_ref, bf16[1024,1024]{1,0:T(8,128)(2,1)} %shift_ref.1, bf16[1024,1024]{1,0:T(8,128)(2,1)} %scale_ref.1, ...), custom_call_target="tpu_custom_call" | custom-call | flops 1048576 | bytes 62914560 | tf_op jit(solution)/shard_map/pallas_call | solution.py:487
  44.5 0.0 copy-start.4
  44.5 1.5 slice_bitcast_fusion.1
  46.0 0.2 pad_maximum_fusion
  46.2 0.7 copy.29
  46.9 0.4 reshape.22
  47.3 0.0 copy-start.1
  47.3 0.0 copy-done.4
  47.3 0.3 convolution_convert_fusion.6
  47.6 0.0 copy-start.3
  47.6 3.1 %convolution_convert_fusion.4 = bf16[32,512]{1,0:T(8,128)(2,1)S(1)} fusion(bf16[32,4096]{1,0:T(8,128)(2,1)S(1)} %copy-done.4, bf16[4096,512]{1,0:T(8,128)(2,1)} %param.25), kind=kOutput, calls=%fused_computation.4 | convolution fusion | flops 134234112 | bytes 4489216 | tf_op jit(solution)/shard_map/dot_general | solution.py:26
  50.7 0.0 copy-done.1
  50.8 0.8 convolution_convert_fusion.3
  51.6 0.0 copy-done.3
  51.6 0.5 convolution_convert_fusion.5
  52.1 0.7 copy.30.low_ref
  52.8 0.0 copy-start
  52.8 0.0 copy-start.2
  52.8 3.7 %convolution_convert_fusion.2.query_ref = bf16[128,512]{1,0:T(8,128)(2,1)} fusion(bf16[128,4096]{1,0:T(8,128)(2,1)S(1)} %bitcast.36, bf16[4096,512]{1,0:T(8,128)(2,1)} %param.24), kind=kOutput, calls=%fused_computation.2 | convolution fusion | flops 536936448 | bytes 5373952 | tf_op jit(solution)/shard_map/dot_general | solution.py:26
  56.5 0.0 copy-done
  56.5 0.0 copy-start.5
  56.5 1.4 convolution_convert_fusion.1.key_ref
  57.9 0.0 copy-done.2
  57.9 1.4 convolution_convert_fusion.value_ref
  59.4 0.0 copy-done.5
  59.4 0.8 copy.31.spike_ref
  60.2 0.6 fusion.1.own_ref
  60.9 23.0 %shard_map.164 = bf16[4,32,1152]{2,1,0:T(8,128)(2,1)} custom-call(bf16[32,1152]{1,0:T(8,128)(2,1)} %fusion.1.own_ref), custom_call_target="tpu_custom_call" | custom-call | flops 1048576 | bytes 20971520 | tf_op jit(solution)/shard_map/pallas_call | solution.py:528
  83.9 23.6 %shard_map.165 = (bf16[2,4,2,64,128]{4,3,2,1,0:T(8,128)(2,1)}, f32[2,4,64,128]{3,2,1,0:T(8,128)}, bf16[2,128,512]{2,1,0:T(8,128)(2,1)}, f32[128,512]{1,0:T(8,128)}) custom-call(bf16[128,512]{1,0:T(8,128)(2,1)} %convolution_convert_fusion.2.query_ref, bf16[128,512]{1,0:T(8,128)(2,1)} %convolution_convert_fusion.1.key_ref, ...), custom_call_target="tpu_custom_call" | custom-call | flops 2281701376 | bytes 4194304 | tf_op jit(solution)/shard_map/pallas_call | solution.py:273
  107.4 16.8 %shard_map.166.normed_ref = bf16[128,512]{1,0:T(8,128)(2,1)} custom-call(bf16[2,4,2,64,128]{4,3,2,1,0:T(8,128)(2,1)} %get-tuple-element.16.maps_ref, f32[2,4,64,128]{3,2,1,0:T(8,128)} %get-tuple-element.17.ctx_ref, bf16[2,128,512]{2,1,0:T(8,128)(2,1)} %get-tuple-element.18.reading_ref, f32[128,512]{1,0:T(8,128)} %get-tuple-element.19.inside_ref, ...), custom_call_target="tpu_custom_call" | custom-call | flops 134217728 | bytes 41943040 | tf_op jit(solution)/shard_map/pallas_call | solution.py:620
  124.2 0.0 all-gather.2.cloned.1.call-done.weight_ref
  124.2 13.3 %shard_map.167 = bf16[32,4096]{1,0:T(8,128)(2,1)} custom-call(bf16[128,512]{1,0:T(8,128)(2,1)} %shard_map.166.normed_ref, bf16[512,4096]{1,0:T(8,128)(2,1)} %all-gather.2.cloned.1.call-done.weight_ref, bf16[32,4096]{1,0:T(8,128)(2,1)} %hidden_ref.3, f32[1,4096]{1,0:T(1,128)} %get-tuple-element.20.gates_ref), custom_call_target="tpu_custom_call" | custom-call | tf_op jit(solution)/shard_map/pallas_call | solution.py:723
  137.6 1.7 %copy.35 = bf16[32,4096]{1,0:T(8,128)(2,1)} copy(bf16[32,4096]{1,0:T(8,128)(2,1)} %shard_map.167) | data formatting | bytes 524288
  (4 shorter events, 0.1 us)
Async XLA Ops:
  6.5 117.7 %all-gather.2.cloned.1.call-start = ((), (), s32[]{:S(2)}) async-start(), calls=%async_computation | async-start | bytes 5242880 | tf_op jit(solution)/shard_map/all_gather | solution.py:776
  44.5 2.8 %copy-start.4 = (bf16[32,4096]{1,0:T(8,128)(2,1)S(1)}, bf16[32,4096]{1,0:T(8,128)(2,1)}, u32[]{:S(2)}) copy-start(bf16[32,4096]{1,0:T(8,128)(2,1)} %get-tuple-element.15) | copy-start | bytes 786436
  47.3 3.5 %copy-start.1 = (bf16[4096,512]{1,0:T(8,128)(2,1)S(1)}, bf16[4096,512]{1,0:T(8,128)(2,1)}, u32[]{:S(2)}) copy-start(bf16[4096,512]{1,0:T(8,128)(2,1)} %param.26) | copy-start | bytes 12582916
  47.6 4.0 %copy-start.3 = (bf16[4,32,4096]{2,1,0:T(8,128)(2,1)S(1)}, bf16[4,32,4096]{2,1,0:T(8,128)(2,1)}, u32[]{:S(2)}) copy-start(bf16[4,32,4096]{2,1,0:T(8,128)(2,1)} %get-tuple-element.13) | copy-start | bytes 3145732
  52.8 3.7 %copy-start = (bf16[4096,512]{1,0:T(8,128)(2,1)S(1)}, bf16[4096,512]{1,0:T(8,128)(2,1)}, u32[]{:S(2)}) copy-start(bf16[4096,512]{1,0:T(8,128)(2,1)} %param.25) | copy-start | bytes 12582916
  52.8 5.2 %copy-start.2 = (bf16[4096,512]{1,0:T(8,128)(2,1)S(1)}, bf16[4096,512]{1,0:T(8,128)(2,1)}, u32[]{:S(2)}) copy-start(bf16[4096,512]{1,0:T(8,128)(2,1)} %param.26) | copy-start | bytes 12582916
  56.5 2.9 %copy-start.5 = (f32[128,8]{0,1:T(8,128)S(1)}, f32[128,8]{0,1:T(8,128)}, u32[]{:S(2)}) copy-start(f32[128,8]{0,1:T(8,128)} %param.31) | copy-start | bytes 12292
Sparse Core Ops, SparseCore 0:
  8.9 101.1 all-gather.1

commit v3 on v2

--- a/solution.py
+++ b/solution.py
@@ -1,5 +1,4 @@
 import functools
-import math
 
 import jax
 import jax.numpy as jnp
@@ -522,7 +521,7 @@
         copy.wait()
 
 
-def spread_call(block):
+def spread_call(block, collective_id):
     count = lax.axis_size("sp")
     dma = pltpu.SemaphoreType.DMA
     return pl.pallas_call(
@@ -531,7 +530,7 @@
         out_specs=VMEM_SPEC,
         out_shape=jax.ShapeDtypeStruct((count,) + block.shape, block.dtype),
         scratch_shapes=[dma((count,)), dma((count,))],
-        compiler_params=pltpu.CompilerParams(collective_id=1, has_side_effects=True),
+        compiler_params=pltpu.CompilerParams(collective_id=collective_id, has_side_effects=True),
         cost_estimate=pl.CostEstimate(
             flops=1 << 20, bytes_accessed=20 << 20, transcendentals=0
         ),
@@ -650,22 +649,28 @@
     mate_recv,
     chip_send,
     chip_recv,
+    mixed_ref,
+    token_ref,
+    token_send,
+    token_recv,
 ):
-    tp_own = lax.axis_index("tp")
+    tp_own, sp_own = lax.axis_index("tp"), lax.axis_index("sp")
     chips = tp_count // 2
     chip, core = tp_own // 2, lax.rem(tp_own, 2)
     mate = {"tp": chip * 2 + 1 - core}
     targets = [{"tp": lax.rem(chip + step, chips) * 2 + core} for step in range(1, chips)]
-    greet([mate] + targets)
     pieces = product_ref.shape[0]
+    token_peers = others("sp", pieces)
+    greet([mate] + targets + token_peers)
     span = product_ref.shape[4]
     height = out_ref.shape[0]
-    shape = (chips, 2, height, span)
     mate_copies = []
     for piece in range(pieces):
-        cols = slice(piece * span, (piece + 1) * span)
+        step = (piece + 1) % pieces
         block = jnp.dot(
-            normed_ref[...], weight_ref[:, cols], preferred_element_type=jnp.float32
+            normed_ref[lax.rem(sp_own + step, pieces)],
+            weight_ref[...],
+            preferred_element_type=jnp.float32,
         ).astype(jnp.bfloat16)
         for place in range(chips):
             for side in range(2):
@@ -697,18 +702,38 @@
             )
             copy.start()
             chip_copies.append(copy)
+    token_copies = []
     for piece in range(pieces):
-        cols = slice(piece * span, (piece + 1) * span)
         mixed = product_ref[piece, core, chip].astype(jnp.float32) + mate_ref[
             piece, chip
         ].astype(jnp.float32)
         for step in range(chips - 1):
             chip_copies[piece * (chips - 1) + step].wait_recv()
             mixed += land_ref[piece, step].astype(jnp.float32)
+        if piece < pieces - 1:
+            mixed_ref[piece] = mixed.astype(jnp.bfloat16)
+            copy = remote(
+                mixed_ref.at[piece],
+                token_ref.at[piece],
+                token_send.at[piece],
+                token_recv.at[piece],
+                token_peers[piece],
+            )
+            copy.start()
+            token_copies.append(copy)
+
+    def finish(source, mixed):
+        cols = pl.ds(pl.multiple_of(source * span, PAIR), span)
         out_ref[:, cols] = (
             hidden_ref[:, cols].astype(jnp.float32) + gates_ref[:, cols] * mixed
         ).astype(out_ref.dtype)
-    for copy in mate_copies + chip_copies:
+
+    finish(sp_own, mixed)
+    for piece, copy in enumerate(token_copies):
+        copy.wait_recv()
+        source = lax.rem(sp_own + pieces - piece - 1, pieces)
+        finish(source, token_ref[piece].astype(jnp.float32))
+    for copy in mate_copies + chip_copies + token_copies:
         copy.wait_send()
 
 
@@ -716,8 +741,8 @@
     tp_count = lax.axis_size("tp")
     chips = tp_count // 2
     height, width = hidden.shape
-    pieces = math.gcd(4, width // PAIR)
-    span = width // pieces
+    pieces = normed.shape[0]
+    span = weight.shape[1]
     dma = pltpu.SemaphoreType.DMA
     vmem = lambda *shape: pltpu.VMEM(shape, jnp.bfloat16)
     return pl.pallas_call(
@@ -734,6 +759,10 @@
             dma((pieces,)),
             dma((pieces, chips - 1)),
             dma((pieces, chips - 1)),
+            vmem(pieces - 1, height, span),
+            vmem(pieces - 1, height, span),
+            dma((pieces,)),
+            dma((pieces,)),
         ],
         compiler_params=pltpu.CompilerParams(collective_id=3, has_side_effects=True),
     )(normed, weight, hidden, gates)
@@ -773,7 +802,6 @@
     down_own = jnp.concatenate(
         [joint_lower_projector[:half], joint_lower_projector[half:]], axis=1
     )
-    out_weight = lax.all_gather(emit_matrix, "sp", axis=1, tiled=True)
     features, ctx_mod, gates, down_all = front_call(
         active,
         adjust_shifting,
@@ -793,7 +821,7 @@
     ctx_joined = jnp.concatenate(
         [ctx_key, ctx_value, jnp.pad(ctx_low, ((0, 0), (0, PAIR - rank)))], axis=1
     )
-    ctx_all = spread_call(ctx_joined).reshape(-1, ctx_joined.shape[1])
+    ctx_all = spread_call(ctx_joined, 1).reshape(-1, ctx_joined.shape[1])
     maps, ctx_state, reading, inside = chain_call(
         stored(product(features, receiver_matrix)),
         stored(product(features, address_matrix)),
@@ -806,7 +834,7 @@
         spike_logfade,
     )
     normed = read_call(maps, ctx_state, reading, inside, group_standard_factor)
-    return emit_call(normed, out_weight, hidden_items, gates)
+    return emit_call(spread_call(normed, 4), emit_matrix, hidden_items, gates)
 
 
 def solution(mesh):

time: 147 us -> 138 us (0.939)
  between operations: 13.6 us -> 0.18 us
  Pallas kernels: 110 us -> 115 us
    pallas_call x1 -> x2, Pallas kernels: 23 us -> 27.7 us  [spread_call(): pl.pallas_call(functools.partial(spread_kernel, count), in_specs=[VMEM_SP...]
    pallas_call x1, Pallas kernels: 13.3 us -> 17.8 us  [emit_call(): pl.pallas_call(functools.partial(emit_kernel, tp_count), in_specs=[VMEM_S...]
    pallas_call x1, Pallas kernels: 33.1 us -> 29.8 us  [front_call(): pl.pallas_call(functools.partial(front_kernel, sp_count, tp_count), in_sp...]
  transfers between devices with their start and end apart: 1 -> 0, of which waited for: 0 -> 0; matrix products, arithmetic and copies ran while one was open for 14% -> 0% of each run, Pallas kernels for 66% -> 0%
where the time goes in v3:
time: 138 us
  Pallas kernels  115 us (83%)
  matrix products  11.3 us (8%)
  local copies, waits for them, and re-layouts  8.36 us (6%)
  other arithmetic  2.39 us (2%)
    pallas_call x1, Pallas kernels, front_call(): pl.pallas_call(functools.partial(front_kernel, sp_count, tp_count), in_sp...  29.8 us
    pallas_call x2, Pallas kernels, spread_call(): pl.pallas_call(functools.partial(spread_kernel, count), in_specs=[VMEM_SP...  27.7 us
    pallas_call x1, Pallas kernels, chain_call(): pl.pallas_call(chain_kernel, grid=(pairs,), in_specs=[columns(rows), colu...  23.5 us
    pallas_call x1, Pallas kernels, emit_call(): pl.pallas_call(functools.partial(emit_kernel, tp_count), in_specs=[VMEM_S...  17.8 us
    pallas_call x1, Pallas kernels, read_call(): pl.pallas_call(functools.partial(read_kernel, count), in_specs=[VMEM_SPEC...  16.5 us
    dot_general x7, matrix products, product(): return jnp.dot(left, right, preferred_element_type=jnp.float32)  11.3 us

profile of v3, /device:TPU:0, one launch (start us, length us, event | category | flops | bytes accessed | tf_op | source)
XLA Modules:
  0.0 137.5 jit_solution(1629310639052660002)
XLA Ops:
  0.0 0.7 stack.30
  0.7 0.7 stack.31
  1.5 0.6 pad_maximum_fusion.2.active_ref
  2.2 0.9 fusion.3
  3.1 0.1 copy.32
  3.2 0.1 copy.33
  3.3 0.8 pad_maximum_fusion.1.down_ref
  4.1 29.8 %shard_map.163 = (bf16[4,32,4096]{2,1,0:T(8,128)(2,1)}, bf16[32,4096]{1,0:T(8,128)(2,1)}, f32[1,4096]{1,0:T(1,128)}, bf16[4,512,128]{2,1,0:T(8,128)(2,1)}) custom-call(bf16[3,16,1024]{2,1,0:T(8,128)(2,1)} %pad_maximum_fusion.2.active_ref, bf16[1024,1024]{1,0:T(8,128)(2,1)} %shift_ref.1, bf16[1024,1024]{1,0:T(8,128)(2,1)} %scale_ref.1, ...), custom_call_target="tpu_custom_call" | custom-call | flops 1048576 | bytes 62914560 | tf_op jit(solution)/shard_map/pallas_call | solution.py:486
  33.9 0.0 copy-start.4
  33.9 1.5 %slice_bitcast_fusion.1 = (bf16[4,1,512,64]{3,2,0,1:T(8,128)(2,1)S(1)}, bf16[4,1,512,64]{3,2,0,1:T(8,128)(2,1)S(1)}) fusion(bf16[4,512,128]{2,1,0:T(8,128)(2,1)} %get-tuple-element.14), kind=kLoop, calls=%fused_computation.9 | loop fusion | bytes 1048576 | tf_op jit(solution)/shard_map/stack | solution.py:816
  35.3 0.2 pad_maximum_fusion
  35.6 0.7 copy.29
  36.2 0.4 reshape.22
  36.6 0.0 copy-start.1
  36.6 0.0 copy-done.4
  36.7 0.3 convolution_convert_fusion.6
  36.9 0.0 copy-start.3
  36.9 3.1 %convolution_convert_fusion.4 = bf16[32,512]{1,0:T(8,128)(2,1)S(1)} fusion(bf16[32,4096]{1,0:T(8,128)(2,1)S(1)} %copy-done.4, bf16[4096,512]{1,0:T(8,128)(2,1)} %param.25), kind=kOutput, calls=%fused_computation.4 | convolution fusion | flops 134234112 | bytes 4489216 | tf_op jit(solution)/shard_map/dot_general | solution.py:25
  40.1 0.0 copy-done.1
  40.1 0.8 convolution_convert_fusion.3
  40.9 0.7 fusion.1.own_ref
  41.6 13.1 %shard_map.164 = bf16[4,32,1152]{2,1,0:T(8,128)(2,1)} custom-call(bf16[32,1152]{1,0:T(8,128)(2,1)} %fusion.1.own_ref), custom_call_target="tpu_custom_call" | custom-call | flops 1048576 | bytes 20971520 | tf_op jit(solution)/shard_map/pallas_call | solution.py:527
  54.7 0.0 copy-done.3
  54.7 0.5 convolution_convert_fusion.5
  55.2 0.7 copy.30.low_ref
  55.9 0.0 copy-start
  55.9 0.0 copy-start.2
  55.9 3.7 %convolution_convert_fusion.2.query_ref = bf16[128,512]{1,0:T(8,128)(2,1)} fusion(bf16[128,4096]{1,0:T(8,128)(2,1)S(1)} %bitcast.36, bf16[4096,512]{1,0:T(8,128)(2,1)} %param.24), kind=kOutput, calls=%fused_computation.2 | convolution fusion | flops 536936448 | bytes 5373952 | tf_op jit(solution)/shard_map/dot_general | solution.py:25
  59.6 0.0 copy-done
  59.6 0.0 copy-start.5
  59.6 1.4 %convolution_convert_fusion.1.key_ref = bf16[128,512]{1,0:T(8,128)(2,1)} fusion(bf16[128,4096]{1,0:T(8,128)(2,1)S(1)} %bitcast.37, bf16[4096,512]{1,0:T(8,128)(2,1)S(1)} %copy-done), kind=kOutput, calls=%fused_computation.1 | convolution fusion | flops 536936448 | bytes 5373952 | tf_op jit(solution)/shard_map/dot_general | solution.py:25
  61.1 0.0 copy-done.2
  61.1 1.4 %convolution_convert_fusion.value_ref = bf16[128,512]{1,0:T(8,128)(2,1)} fusion(bf16[128,4096]{1,0:T(8,128)(2,1)S(1)} %bitcast.38, bf16[4096,512]{1,0:T(8,128)(2,1)S(1)} %copy-done.2), kind=kOutput, calls=%fused_computation | convolution fusion | flops 536936448 | bytes 5373952 | tf_op jit(solution)/shard_map/dot_general | solution.py:25
  62.5 0.0 copy-done.5
  62.5 0.8 copy.31.spike_ref
  63.3 23.5 %shard_map.165 = (bf16[2,4,2,64,128]{4,3,2,1,0:T(8,128)(2,1)}, f32[2,4,64,128]{3,2,1,0:T(8,128)}, bf16[2,128,512]{2,1,0:T(8,128)(2,1)}, f32[128,512]{1,0:T(8,128)}) custom-call(bf16[128,512]{1,0:T(8,128)(2,1)} %convolution_convert_fusion.2.query_ref, bf16[128,512]{1,0:T(8,128)(2,1)} %convolution_convert_fusion.1.key_ref, ...), custom_call_target="tpu_custom_call" | custom-call | flops 2281701376 | bytes 4194304 | tf_op jit(solution)/shard_map/pallas_call | solution.py:272
  86.9 16.5 %shard_map.166.own_ref = bf16[128,512]{1,0:T(8,128)(2,1)} custom-call(bf16[2,4,2,64,128]{4,3,2,1,0:T(8,128)(2,1)} %get-tuple-element.16.maps_ref, f32[2,4,64,128]{3,2,1,0:T(8,128)} %get-tuple-element.17.ctx_ref, bf16[2,128,512]{2,1,0:T(8,128)(2,1)} %get-tuple-element.18.reading_ref, f32[128,512]{1,0:T(8,128)} %get-tuple-element.19.inside_ref, f32[1,512]{1,0:T(1,128)} %bitcast.45), custom_call_target="tpu_custom_call" | custom-call | flops 134217728 | bytes 41943040 | tf_op jit(solution)/shard_map/pallas_call | solution.py:619
  103.4 14.6 %shard_map.167.normed_ref = bf16[4,128,512]{2,1,0:T(8,128)(2,1)} custom-call(bf16[128,512]{1,0:T(8,128)(2,1)} %shard_map.166.own_ref), custom_call_target="tpu_custom_call" | custom-call | flops 1048576 | bytes 20971520 | tf_op jit(solution)/shard_map/pallas_call | solution.py:527
  118.0 17.8 %shard_map.168 = bf16[32,4096]{1,0:T(8,128)(2,1)} custom-call(bf16[4,128,512]{2,1,0:T(8,128)(2,1)} %shard_map.167.normed_ref, bf16[512,1024]{1,0:T(8,128)(2,1)} %weight_ref.1, bf16[32,4096]{1,0:T(8,128)(2,1)} %hidden_ref.3, f32[1,4096]{1,0:T(1,128)} %get-tuple-element.20.gates_ref), custom_call_target="tpu_custom_call" | custom-call | tf_op jit(solution)/shard_map/pallas_call | solution.py:748
  135.9 1.7 %copy.35 = bf16[32,4096]{1,0:T(8,128)(2,1)} copy(bf16[32,4096]{1,0:T(8,128)(2,1)} %shard_map.168) | data formatting | bytes 524288
  (4 shorter events, 0.1 us)
Async XLA Ops:
  33.9 2.8 %copy-start.4 = (bf16[32,4096]{1,0:T(8,128)(2,1)S(1)}, bf16[32,4096]{1,0:T(8,128)(2,1)}, u32[]{:S(2)}) copy-start(bf16[32,4096]{1,0:T(8,128)(2,1)} %get-tuple-element.15) | copy-start | bytes 786436
  36.6 3.5 %copy-start.1 = (bf16[4096,512]{1,0:T(8,128)(2,1)S(1)}, bf16[4096,512]{1,0:T(8,128)(2,1)}, u32[]{:S(2)}) copy-start(bf16[4096,512]{1,0:T(8,128)(2,1)} %param.26) | copy-start | bytes 12582916
  36.9 17.8 %copy-start.3 = (bf16[4,32,4096]{2,1,0:T(8,128)(2,1)S(1)}, bf16[4,32,4096]{2,1,0:T(8,128)(2,1)}, u32[]{:S(2)}) copy-start(bf16[4,32,4096]{2,1,0:T(8,128)(2,1)} %get-tuple-element.13) | copy-start | bytes 3145732
  55.9 3.7 %copy-start = (bf16[4096,512]{1,0:T(8,128)(2,1)S(1)}, bf16[4096,512]{1,0:T(8,128)(2,1)}, u32[]{:S(2)}) copy-start(bf16[4096,512]{1,0:T(8,128)(2,1)} %param.25) | copy-start | bytes 12582916
  55.9 5.1 %copy-start.2 = (bf16[4096,512]{1,0:T(8,128)(2,1)S(1)}, bf16[4096,512]{1,0:T(8,128)(2,1)}, u32[]{:S(2)}) copy-start(bf16[4096,512]{1,0:T(8,128)(2,1)} %param.26) | copy-start | bytes 12582916
  59.6 2.9 %copy-start.5 = (f32[128,8]{0,1:T(8,128)S(1)}, f32[128,8]{0,1:T(8,128)}, u32[]{:S(2)}) copy-start(f32[128,8]{0,1:T(8,128)} %param.31) | copy-start | bytes 12292
